TPU v7x, 32 devices: a whole 2x2x4 slice. The times are simulated.
32 devices in a mesh: sp: 8 (over z, y), tp: 4 (over x, core).
Axes of the slice: x: 2, y: 2, z: 4, core: 2. Of those that a mesh axis runs over, the one named last changes fastest.
Arguments:
- cotangent: bfloat16 [1536, 4096], P('sp'), may hold values from -6 to 6
- moe_input: bfloat16 [1536, 4096], P('sp'), may hold values from -6 to 6
- routes: int32 [1536, 2], P('sp'), may hold values from 0 to 7, all different within a row; in each aligned block of 192 rows (0 to 191, 192 to 383, ...) at most 96 rows name the same one
- route_weight: float32 [1536, 2], P('sp'), may hold values from 0.3 to 1.7
- conv_input: bfloat16 [1536, 2048], P('sp', 'tp'), may hold values from -6 to 6
- input_gate: bfloat16 [1536, 2048], P('sp', 'tp'), may hold values from -6 to 6
- output_gate: bfloat16 [1536, 2048], P('sp', 'tp'), may hold values from -6 to 6
- conv_output: bfloat16 [1536, 2048], P('sp', 'tp'), may hold values from -6 to 6
- taps: float32 [3, 2048], P(None, 'tp'), may hold values from -3 to 3
- w_out: bfloat16 [4096, 2048], P(None, 'tp'), may hold values from -0.125 to 0.125
- w_gate: bfloat16 [8, 4096, 1024], P('sp', None, 'tp'), may hold values from -0.09375 to 0.09375
- w_up: bfloat16 [8, 4096, 1024], P('sp', None, 'tp'), may hold values from -0.09375 to 0.09375
- w_down: bfloat16 [8, 1024, 4096], P('sp', 'tp'), may hold values from -0.1875 to 0.1875
Outputs:
- grad_w_gate: bfloat16 [8, 4096, 1024], P('sp', None, 'tp')
- grad_w_up: bfloat16 [8, 4096, 1024], P('sp', None, 'tp')
- grad_w_down: bfloat16 [8, 1024, 4096], P('sp', 'tp')
- grad_w_out: float32 [4096, 2048], P('sp', 'tp')
- grad_conv_input: bfloat16 [1536, 2048], P('sp', 'tp')
- grad_input_gate: bfloat16 [1536, 2048], P('sp', 'tp')
- grad_output_gate: bfloat16 [1536, 2048], P('sp', 'tp')
Inputs may be any that keep to these rules, and one draw needn't show every extreme that they name: `routes`: each row names 2 different experts. Among the rows of one index of sp no expert is named by more than 96 rows, and in every draw some expert is named by exactly 96 rows of some index.
All inputs are finite; a program needn't handle non-finite values.
Results may differ from a plain program's by a relative error of at most 0.0065.
Values may be sent and summed in bfloat16 or wider, within the bound.
A program may use at most 192 MiB of HBM per device.

v0:
```python
import jax
import jax.numpy as jnp
from jax import lax
from jax.sharding import PartitionSpec as P

ROW_CHUNKS = 1


def from_behind(value, axis, steps):
    count = lax.axis_size(axis)
    leading, last = (max(0, -steps), min(count, count - steps))
    return lax.ppermute(value, axis, [(source, source + steps) for source in range(leading, last)])


def silu_parts(gate_proj):
    sigmoid_gate = jax.nn.sigmoid(gate_proj)
    activated = gate_proj * sigmoid_gate
    slope = sigmoid_gate * (1.0 + gate_proj * (1.0 - sigmoid_gate))
    return (activated, slope)


def expert_backward(scaled_rows, input_rows, gate_weight, up_weight, down_weight):
    gate_proj = jnp.dot(input_rows, gate_weight, preferred_element_type=jnp.float32)
    up_proj = jnp.dot(input_rows, up_weight, preferred_element_type=jnp.float32)
    activated, slope = silu_parts(gate_proj)
    hidden = (activated * up_proj).astype(jnp.bfloat16)
    grad_down = lax.dot_general(
        hidden, scaled_rows, (((0,), (0,)), ((), ())), preferred_element_type=jnp.float32
    )
    grad_hidden = lax.dot_general(
        scaled_rows, down_weight, (((1,), (1,)), ((), ())), preferred_element_type=jnp.float32
    )
    grad_gate = (grad_hidden * up_proj * slope).astype(jnp.bfloat16)
    grad_up = (grad_hidden * activated).astype(jnp.bfloat16)
    gate_wgrad = lax.dot_general(
        input_rows, grad_gate, (((0,), (0,)), ((), ())), preferred_element_type=jnp.float32
    )
    up_wgrad = lax.dot_general(
        input_rows, grad_up, (((0,), (0,)), ((), ())), preferred_element_type=jnp.float32
    )
    return (gate_wgrad, up_wgrad, grad_down, grad_gate, grad_up)


def row_gradient(grad_gate, grad_up, gate_weight, up_weight):
    row_part = lax.dot_general(
        grad_gate, gate_weight, (((1,), (1,)), ((), ())), preferred_element_type=jnp.float32
    )
    return row_part + lax.dot_general(
        grad_up, up_weight, (((1,), (1,)), ((), ())), preferred_element_type=jnp.float32
    )


def by_piece(value, axis, blocks, shares):
    before, after = (value.shape[:axis], value.shape[axis + 1 :])
    piece = value.shape[axis] // (blocks * shares)
    value = value.reshape(before + (blocks, shares, piece) + after)
    return jnp.swapaxes(value, axis, axis + 1).reshape(before + (-1,) + after)


def slot_masks(routes, route_weight, experts, capacity):
    tok_rows = routes.shape[0]
    names = jnp.arange(experts, dtype=jnp.int32)
    hits = routes[None, :, :] == names[:, None, None]
    chosen = jnp.any(hits, axis=2)
    weight = jnp.sum(jnp.where(hits, route_weight[None], 0.0), axis=2)
    order = jnp.arange(tok_rows, dtype=jnp.int32)
    before = (order[:, None] < order[None, :]).astype(jnp.bfloat16)
    rank = jnp.dot(chosen.astype(jnp.bfloat16), before, preferred_element_type=jnp.float32)
    rank = jnp.where(chosen, rank.astype(jnp.int32), -1)
    slots = jnp.arange(capacity, dtype=jnp.int32)
    placed = rank[:, None, :] == slots[None, :, None]
    slot_weight = jnp.sum(jnp.where(placed, weight[:, None, :], 0.0), axis=2, keepdims=True)
    placed = placed.astype(jnp.bfloat16).reshape(experts * capacity, tok_rows)
    return (placed, slot_weight.reshape(experts * capacity, 1))


def per_device(
    cotangent,
    moe_input,
    routes,
    route_weight,
    conv_input,
    input_gate,
    output_gate,
    conv_output,
    taps,
    w_out,
    w_gate,
    w_up,
    w_down,
):
    experts = lax.axis_size("sp")
    tp_size = lax.axis_size("tp")
    tok_rows, top_k = routes.shape
    model_width = cotangent.shape[1]
    capacity = max(2, 2 * tok_rows * top_k // experts)
    part_width = model_width // tp_size
    tp_index = lax.axis_index("tp")
    mixed = (output_gate.astype(jnp.float32) * conv_output.astype(jnp.float32)).astype(jnp.bfloat16)
    placed, slot_weight = slot_masks(routes, route_weight, experts, capacity)
    cot_cols = lax.dynamic_slice_in_dim(cotangent, tp_index * part_width, part_width, 1)
    inp_cols = lax.dynamic_slice_in_dim(moe_input, tp_index * part_width, part_width, 1)
    send_inputs = jnp.dot(placed, inp_cols, preferred_element_type=jnp.float32).astype(jnp.bfloat16)
    send_scaled = (
        slot_weight * jnp.dot(placed, cot_cols, preferred_element_type=jnp.float32)
    ).astype(jnp.bfloat16)

    gate_turned = by_piece(w_gate[0], 0, experts, tp_size)
    up_turned = by_piece(w_up[0], 0, experts, tp_size)
    out_turned = by_piece(w_out, 0, experts, tp_size)
    piece = part_width // experts
    cot_share = cotangent.reshape(tok_rows, experts, tp_size, piece)
    cot_share = lax.dynamic_index_in_dim(cot_share, tp_index, 2, keepdims=False)
    cot_share = cot_share.reshape(tok_rows, part_width)

    def over_sp(value):
        return lax.all_to_all(value, "sp", split_axis=0, concat_axis=0, tiled=True)

    part_inputs = over_sp(send_inputs.reshape(experts, capacity, part_width))
    part_inputs, send_scaled, gate_turned, up_turned, out_turned = lax.optimization_barrier(
        (part_inputs, send_scaled, gate_turned, up_turned, out_turned)
    )
    input_rows = lax.all_gather(part_inputs, "tp", axis=2, tiled=True).reshape(-1, model_width)
    part_scaled = over_sp(send_scaled.reshape(experts, capacity, part_width))
    part_scaled, mixed = lax.optimization_barrier((part_scaled, mixed))
    scaled_rows = lax.all_gather(part_scaled, "tp", axis=2, tiled=True).reshape(-1, model_width)
    mixed_all = over_sp(jnp.broadcast_to(mixed[None], (experts,) + mixed.shape))
    mixed_all = mixed_all.reshape(experts * tok_rows, -1)
    gate_wgrad, up_wgrad, grad_down, grad_gate, grad_up = expert_backward(
        scaled_rows, input_rows, w_gate[0], w_up[0], w_down[0]
    )
    chunks = ROW_CHUNKS if capacity % ROW_CHUNKS == 0 else 1
    step = capacity // chunks
    hidden_units = grad_gate.shape[1]
    shares = []
    for chunk in range(chunks):
        some = [
            value.reshape(experts, capacity, hidden_units)[:, chunk * step : (chunk + 1) * step]
            for value in (grad_gate, grad_up)
        ]
        some = [value.reshape(experts * step, hidden_units) for value in some]
        row_part = row_gradient(some[0], some[1], gate_turned, up_turned).astype(jnp.bfloat16)
        shares.append(lax.psum_scatter(row_part, "tp", scatter_dimension=1, tiled=True))
    gate_wgrad, up_wgrad, grad_down, mixed_all, shares[-1] = lax.optimization_barrier(
        (
            gate_wgrad.astype(jnp.bfloat16),
            up_wgrad.astype(jnp.bfloat16),
            grad_down.astype(jnp.bfloat16),
            mixed_all,
            shares[-1],
        )
    )
    placed = placed.reshape(experts, capacity, tok_rows)
    route_sum = cot_share.astype(jnp.float32)
    for chunk in range(chunks):
        returned = over_sp(shares[chunk].reshape(experts, step, part_width))
        chosen = placed[:, chunk * step : (chunk + 1) * step].reshape(experts * step, tok_rows)
        route_sum = route_sum + lax.dot_general(
            chosen,
            returned.reshape(experts * step, part_width),
            (((0,), (0,)), ((), ())),
            preferred_element_type=jnp.float32,
        )
    resid_part = route_sum.astype(jnp.bfloat16)
    resid_grad = lax.all_gather(resid_part, "tp", axis=1, tiled=True)
    own = over_sp(jnp.swapaxes(resid_part.reshape(tok_rows, experts, piece), 0, 1))
    resid_cols = lax.all_gather(own, "tp", axis=2, tiled=True)
    resid_cols = resid_cols.reshape(experts * tok_rows, model_width // experts)
    grad_w_out = lax.dot_general(
        resid_cols, mixed_all, (((0,), (0,)), ((), ())), preferred_element_type=jnp.float32
    )
    grad_mixed = jnp.dot(resid_grad, out_turned, preferred_element_type=jnp.float32)
    grad_output_gate = (grad_mixed * conv_output.astype(jnp.float32)).astype(jnp.bfloat16)
    grad_conv = grad_mixed * output_gate.astype(jnp.float32)
    following = from_behind(grad_conv[:2], "sp", -1)
    extended = jnp.concatenate([grad_conv, following], axis=0)
    grad_g = (
        taps[2] * extended[:tok_rows]
        + taps[1] * extended[1 : tok_rows + 1]
        + taps[0] * extended[2:]
    )
    grad_conv_input = (grad_g * input_gate.astype(jnp.float32)).astype(jnp.bfloat16)
    grad_input_gate = (grad_g * conv_input.astype(jnp.float32)).astype(jnp.bfloat16)
    return (
        gate_wgrad.astype(jnp.bfloat16)[None],
        up_wgrad.astype(jnp.bfloat16)[None],
        grad_down.astype(jnp.bfloat16)[None],
        grad_w_out,
        grad_conv_input,
        grad_input_gate,
        grad_output_gate,
    )


def solution(mesh):
    return jax.shard_map(
        per_device,
        mesh=mesh,
        in_specs=(
            P("sp", None),
            P("sp", None),
            P("sp", None),
            P("sp", None),
            P("sp", "tp"),
            P("sp", "tp"),
            P("sp", "tp"),
            P("sp", "tp"),
            P(None, "tp"),
            P(None, "tp"),
            P("sp", None, "tp"),
            P("sp", None, "tp"),
            P("sp", "tp", None),
        ),
        out_specs=(
            P("sp", None, "tp"),
            P("sp", None, "tp"),
            P("sp", "tp", None),
            P("sp", "tp"),
            P("sp", "tp"),
            P("sp", "tp"),
            P("sp", "tp"),
        ),
        check_vma=False,
    )
```

profile of v0, /device:TPU:0, one launch (start us, length us, event | category | flops | bytes accessed | tf_op | source)
XLA Modules:
  0.0 315.1 jit_solution(14092271750652960871)
XLA Ops:
  9.6 2.8 convolution_convert_fusion.3
  12.4 7.4 %all-to-all-start = ((bf16[8,96,1024]{2,1,0:T(8,128)(2,1)}), bf16[8,96,1024]{2,1,0:T(8,128)(2,1)}, u32[]{:S(2)}, u32[]{:S(2)}) async-start(bf16[8,96,1024]{2,1,0:T(8,128)(2,1)} %bitcast.80), calls=%async_computation | async-start | bytes 3145728 | tf_op jit(solution)/shard_map/all_to_all | solution.py:117
  20.7 3.3 %copy.40 = bf16[4,8,128,256]{3,2,1,0:T(8,128)(2,1)} copy(bf16[4,8,128,256]{3,2,0,1:T(8,128)(2,1)} %bitcast.83) | data formatting | bytes 4194304 | tf_op jit(solution)/shard_map/transpose | solution.py:57
  25.4 1.5 copy-done.5
  26.9 2.5 copy.42
  29.4 2.8 multiply_convert_fusion
  32.2 24.8 %all-to-all-done = bf16[8,96,1024]{2,1,0:T(8,128)(2,1)} async-done(((bf16[8,96,1024]{2,1,0:T(8,128)(2,1)}), bf16[8,96,1024]{2,1,0:T(8,128)(2,1)}, u32[]{:S(2)}, u32[]{:S(2)}) %all-to-all-start) | async-done | bytes 1572896 | tf_op jit(solution)/shard_map/all_to_all | solution.py:117
  57.0 4.5 %all-to-all-start.1 = ((bf16[8,96,1024]{2,1,0:T(8,128)(2,1)}), bf16[8,96,1024]{2,1,0:T(8,128)(2,1)}, u32[]{:S(2)}, u32[]{:S(2)}) async-start(bf16[8,96,1024]{2,1,0:T(8,128)(2,1)} %bitcast.79), calls=%async_computation.1 | async-start | bytes 3145728 | tf_op jit(solution)/shard_map/all_to_all | solution.py:117
  61.6 36.5 %all-to-all-done.1 = bf16[8,96,1024]{2,1,0:T(8,128)(2,1)} async-done(((bf16[8,96,1024]{2,1,0:T(8,128)(2,1)}), bf16[8,96,1024]{2,1,0:T(8,128)(2,1)}, u32[]{:S(2)}, u32[]{:S(2)}) %all-to-all-start.1) | async-done | bytes 1572896 | tf_op jit(solution)/shard_map/all_to_all | solution.py:117
  98.3 4.2 %all-gather.5.cloned.1.call-done = bf16[8,96,4096]{2,1,0:T(8,128)(2,1)} async-done(((bf16[8,96,1024]{2,1,0:T(8,128)(2,1)}), bf16[8,96,4096]{2,1,0:T(8,128)(2,1)}) %all-gather.5.cloned.1.call-update) | async-done | bytes 6291472 | tf_op jit(solution)/shard_map/all_gather | solution.py:123
  102.6 6.2 %fusion = f32[768,256]{1,0:T(8,128)} fusion(bf16[768,4096]{1,0:T(8,128)(2,1)} %bitcast.91, bf16[1,4096,256]{2,1,0:T(8,128)(2,1)} %param.23), kind=kOutput, calls=%fused_computation.5 | convolution fusion | flops 1610612736 | bytes 9175040 | tf_op jit(solution)/shard_map/dot_general | solution.py:23
  108.8 2.7 fusion.2
  111.5 39.0 %all-gather.7.cloned.1.call-done = bf16[8,96,4096]{2,1,0:T(8,128)(2,1)} async-done(((bf16[8,96,1024]{2,1,0:T(8,128)(2,1)}), bf16[8,96,4096]{2,1,0:T(8,128)(2,1)}) %all-gather.7.cloned.1.call-update) | async-done | bytes 6291472 | tf_op jit(solution)/shard_map/all_gather | solution.py:126
  150.5 5.3 %multiply_convert_fusion.2 = (bf16[768,256]{1,0:T(8,128)(2,1)S(1)}, bf16[768,256]{1,0:T(8,128)(2,1)S(1)}) fusion(f32[768,256]{1,0:T(8,128)} %fusion, f32[768,256]{1,0:T(8,128)} %fusion.2, bf16[768,4096]{1,0:T(8,128)(2,1)} %bitcast.95, bf16[1,256,4096]{2,1,0:T(8,128)(2,1)S(1)} %copy-done), kind=kOutput, calls=%fused_computation.18 | convolution fusion | flops 1613168640 | bytes 10747904 | tf_op jit(solution)/shard_map/dot_general | solution.py:30
  155.8 1.8 fusion.27
  157.7 4.5 %add_convert_fusion = bf16[768,4096]{1,0:T(8,128)(2,1)} fusion(f32[768,4096]{1,0:T(8,128)S(1)} %fusion.27, bf16[768,256]{1,0:T(8,128)(2,1)S(1)} %get-tuple-element.33, bf16[4096,256]{1,0:T(8,128)(2,1)S(1)} %bitcast.78), kind=kOutput, calls=%fused_computation | convolution fusion | flops 1616904192 | bytes 21364736 | tf_op jit(solution)/shard_map/dot_general | solution.py:48
  163.5 5.5 %all-to-all-start.2 = ((bf16[8,192,512]{2,1,0:T(8,128)(2,1)}), bf16[8,192,512]{2,1,0:T(8,128)(2,1)S(1)}, u32[]{:S(2)}, u32[]{:S(2)}) async-start(bf16[8,192,512]{2,1,0:T(8,128)(2,1)} %broadcast_in_dim.56), calls=%async_computation.2 | async-start | bytes 3145728 | tf_op jit(solution)/shard_map/all_to_all | solution.py:117
  169.1 7.6 %convolution_convert_fusion.2 = bf16[4096,256]{1,0:T(8,128)(2,1)} fusion(bf16[768,4096]{1,0:T(8,128)(2,1)} %bitcast.92, bf16[768,256]{1,0:T(8,128)(2,1)S(1)} %get-tuple-element.34), kind=kOutput, calls=%fused_computation.3 | convolution fusion | flops 1611661312 | bytes 8781824 | tf_op jit(solution)/shard_map/dot_general | solution.py:35
  176.7 6.1 %convolution_convert_fusion.1 = bf16[4096,256]{1,0:T(8,128)(2,1)} fusion(bf16[768,4096]{1,0:T(8,128)(2,1)} %bitcast.93, bf16[768,256]{1,0:T(8,128)(2,1)S(1)} %copy-done.13), kind=kOutput, calls=%fused_computation.2 | convolution fusion | flops 1611661312 | bytes 8781824 | tf_op jit(solution)/shard_map/dot_general | solution.py:38
  182.8 3.2 %convolution_convert_fusion = bf16[256,4096]{1,0:T(8,128)(2,1)} fusion(bf16[768,4096]{1,0:T(8,128)(2,1)S(1)} %bitcast.98, f32[768,256]{1,0:T(8,128)S(1)} %copy-done.21, f32[768,256]{1,0:T(8,128)S(1)} %copy-done.20), kind=kOutput, calls=%fused_computation.1 | convolution fusion | flops 1612840960 | bytes 9961472 | tf_op jit(solution)/shard_map/dot_general | solution.py:27
  186.0 20.4 %all-to-all-done.2 = bf16[8,192,512]{2,1,0:T(8,128)(2,1)S(1)} async-done(((bf16[8,192,512]{2,1,0:T(8,128)(2,1)}), bf16[8,192,512]{2,1,0:T(8,128)(2,1)S(1)}, u32[]{:S(2)}, u32[]{:S(2)}) %all-to-all-start.2) | async-done | bytes 1572896 | tf_op jit(solution)/shard_map/all_to_all | solution.py:117
  206.5 13.8 %reduce-scatter.2.cloned.1.call-done = bf16[768,1024]{1,0:T(8,128)(2,1)} async-done(((bf16[768,4096]{1,0:T(8,128)(2,1)}), bf16[768,1024]{1,0:T(8,128)(2,1)}) %reduce-scatter.2.cloned.1.call-update) | async-done | bytes 1572880 | tf_op jit(solution)/shard_map/reduce_scatter | solution.py:143
  220.2 5.5 %all-to-all-start.3 = ((bf16[8,96,1024]{2,1,0:T(8,128)(2,1)}), bf16[8,96,1024]{2,1,0:T(8,128)(2,1)}, u32[]{:S(2)}, u32[]{:S(2)}) async-start(bf16[8,96,1024]{2,1,0:T(8,128)(2,1)} %bitcast.85), calls=%async_computation.4 | async-start | bytes 3145728 | tf_op jit(solution)/shard_map/all_to_all | solution.py:117
  225.8 3.8 %reshape.76 = bf16[192,8,4,128]{3,2,1,0:T(4,128)(2,1)} reshape(bf16[192,4096]{1,0:T(8,128)(2,1)} %param.13) | data formatting | bytes 3145728 | tf_op jit(solution)/shard_map/reshape | solution.py:112
  229.6 2.2 constant_dynamic-slice_fusion
  232.2 30.6 %all-to-all-done.3 = bf16[8,96,1024]{2,1,0:T(8,128)(2,1)} async-done(((bf16[8,96,1024]{2,1,0:T(8,128)(2,1)}), bf16[8,96,1024]{2,1,0:T(8,128)(2,1)}, u32[]{:S(2)}, u32[]{:S(2)}) %all-to-all-start.3) | async-done | bytes 1572896 | tf_op jit(solution)/shard_map/all_to_all | solution.py:117
  262.7 2.7 fusion.7
  266.6 15.8 %all_to_all.25 = bf16[8,192,128]{2,1,0:T(8,128)(2,1)} all-to-all(bf16[8,192,128]{2,1,0:T(8,128)(2,1)S(1)} %bitcast_bitcast_fusion), channel_id=1, replica_groups=mesh['sp'=8,'tp'=4] {'sp'}, dimensions={0} | all-to-all | bytes 786432 | tf_op jit(solution)/shard_map/all_to_all | solution.py:117
  283.4 4.3 %fusion.16 = (bf16[192,512]{1,0:T(8,128)(2,1)}, f32[192,512]{1,0:T(8,128)S(1)}) fusion(bf16[192,512]{1,0:T(8,128)(2,1)S(1)} %copy-done.10, bf16[192,512]{1,0:T(8,128)(2,1)S(1)} %copy-done.11, bf16[192,4096]{1,0:T(8,128)(2,1)} %all-gather.11.cloned.1.call-done, bf16[4096,512]{1,0:T(8,128)(2,1)} %bitcast.76), kind=kOutput, calls=%fused_computation.35 | convolution fusion | flops 805797888 | bytes 6750208 | tf_op jit(solution)/shard_map/dot_general | solution.py:172
  289.0 4.2 %collective-permute-done = f32[2,512]{1,0:T(2,128)S(1)} collective-permute-done((f32[2,512]{1,0:T(2,128)S(1)}, f32[2,512]{1,0:T(2,128)S(1)}, u32[]{:S(2)}, u32[]{:S(2)}) %collective-permute-start) | collective-permute-done | bytes 4128 | tf_op jit(solution)/shard_map/ppermute | solution.py:12
  294.7 9.9 %all-gather.9.cloned.1.call-done = bf16[8,192,512]{2,1,0:T(8,128)(2,1)} async-done(((bf16[8,192,128]{2,1,0:T(8,128)(2,1)}), bf16[8,192,512]{2,1,0:T(8,128)(2,1)}) %all-gather.9.cloned.1.call-update) | async-done | bytes 1572880 | tf_op jit(solution)/shard_map/all_gather | solution.py:167
  304.6 4.0 %fusion.28 = f32[512,512]{1,0:T(8,128)} fusion(bf16[1536,512]{1,0:T(8,128)(2,1)} %bitcast.86, bf16[1536,512]{1,0:T(8,128)(2,1)} %bitcast.81), kind=kOutput, calls=%fused_computation.55 | convolution fusion | flops 805306368 | bytes 4194304 | tf_op jit(solution)/shard_map/dot_general | solution.py:169
  (82 shorter events, 11.8 us)
Async XLA Ops:
  7.2 143.3 %copy-start = (bf16[1,256,4096]{2,1,0:T(8,128)(2,1)S(1)}, bf16[1,256,4096]{2,1,0:T(8,128)(2,1)}, u32[]{:S(2)}) copy-start(bf16[1,256,4096]{2,1,0:T(8,128)(2,1)} %param.25) | copy-start | bytes 6291460
  12.4 7.5 %copy-start.16 = (s32[192,2]{0,1:T(2,128)S(1)}, s32[192,2]{0,1:T(2,128)}, u32[]{:S(2)}) copy-start(s32[192,2]{0,1:T(2,128)} %param.15) | copy-start | bytes 4612
  12.4 7.5 %copy-start.18 = (f32[192,2]{0,1:T(2,128)S(1)}, f32[192,2]{0,1:T(2,128)}, u32[]{:S(2)}) copy-start(f32[192,2]{0,1:T(2,128)} %param.16) | copy-start | bytes 4612
  12.4 7.6 %copy-start.9 = (s32[8,192]{0,1:T(8,128)S(1)}, s32[8,192]{0,1:T(8,128)}, u32[]{:S(2)}) copy-start(s32[8,192]{0,1:T(8,128)} %copy-done.8) | copy-start | bytes 18436
  12.4 44.5 %all-to-all-start = ((bf16[8,96,1024]{2,1,0:T(8,128)(2,1)}), bf16[8,96,1024]{2,1,0:T(8,128)(2,1)}, u32[]{:S(2)}, u32[]{:S(2)}) async-start(bf16[8,96,1024]{2,1,0:T(8,128)(2,1)} %bitcast.80), calls=%async_computation | async-start | bytes 3145728 | tf_op jit(solution)/shard_map/all_to_all | solution.py:117
  19.9 82.7 %all-gather.5.cloned.1.call-start = ((), (), s32[]{:S(2)}) async-start(), calls=%async_computation.6 | async-start | bytes 7864320 | tf_op jit(solution)/shard_map/all_gather | solution.py:123
  20.7 3.3 %copy-start.6 = (bf16[1,4096,256]{2,1,0:T(8,128)(2,1)S(1)}, bf16[1,4096,256]{2,1,0:T(8,128)(2,1)}, u32[]{:S(2)}) copy-start(bf16[1,4096,256]{2,1,0:T(8,128)(2,1)} %param.24) | copy-start | bytes 6291460
  24.0 2.9 copy-start.5
  57.0 4.5 %copy-start.10 = (bf16[192,512]{1,0:T(8,128)(2,1)S(1)}, bf16[192,512]{1,0:T(8,128)(2,1)}, u32[]{:S(2)}) copy-start(bf16[192,512]{1,0:T(8,128)(2,1)} %param.20) | copy-start | bytes 589828
  57.0 4.5 %copy-start.11 = (bf16[192,512]{1,0:T(8,128)(2,1)S(1)}, bf16[192,512]{1,0:T(8,128)(2,1)}, u32[]{:S(2)}) copy-start(bf16[192,512]{1,0:T(8,128)(2,1)} %param.19) | copy-start | bytes 589828
  57.0 41.1 %all-to-all-start.1 = ((bf16[8,96,1024]{2,1,0:T(8,128)(2,1)}), bf16[8,96,1024]{2,1,0:T(8,128)(2,1)}, u32[]{:S(2)}, u32[]{:S(2)}) async-start(bf16[8,96,1024]{2,1,0:T(8,128)(2,1)} %bitcast.79), calls=%async_computation.1 | async-start | bytes 3145728 | tf_op jit(solution)/shard_map/all_to_all | solution.py:117
  61.5 89.0 %all-gather.7.cloned.1.call-start = ((), (), s32[]{:S(2)}) async-start(), calls=%async_computation.7 | async-start | bytes 7864320 | tf_op jit(solution)/shard_map/all_gather | solution.py:126
  98.1 122.1 %reduce-scatter.2.cloned.1.call-start = ((), (), s32[]{:S(2)}) async-start(), calls=%async_computation.8 | async-start | bytes 7864320 | tf_op jit(solution)/shard_map/reduce_scatter | solution.py:143
  102.6 6.2 %copy-start.7 = (bf16[1,4096,256]{2,1,0:T(8,128)(2,1)S(1)}, bf16[1,4096,256]{2,1,0:T(8,128)(2,1)}, u32[]{:S(2)}) copy-start(bf16[1,4096,256]{2,1,0:T(8,128)(2,1)} %param.24) | copy-start | bytes 6291460
  102.6 6.2 %copy-start.19 = (bf16[8,96,4096]{2,1,0:T(8,128)(2,1)S(1)}, bf16[8,96,4096]{2,1,0:T(8,128)(2,1)}, u32[]{:S(2)}) copy-start(bf16[8,96,4096]{2,1,0:T(8,128)(2,1)} %all-gather.5.cloned.1.call-done) | copy-start | bytes 18874372
  150.5 5.3 %copy-start.2 = (bf16[4,8,128,256]{3,2,1,0:T(8,128)(2,1)S(1)}, bf16[4,8,128,256]{3,2,1,0:T(8,128)(2,1)}, u32[]{:S(2)}) copy-start(bf16[4,8,128,256]{3,2,1,0:T(8,128)(2,1)} %copy.40) | copy-start | bytes 6291460
  155.8 1.9 copy-start.12
  163.5 42.9 %all-to-all-start.2 = ((bf16[8,192,512]{2,1,0:T(8,128)(2,1)}), bf16[8,192,512]{2,1,0:T(8,128)(2,1)S(1)}, u32[]{:S(2)}, u32[]{:S(2)}) async-start(bf16[8,192,512]{2,1,0:T(8,128)(2,1)} %broadcast_in_dim.56), calls=%async_computation.2 | async-start | bytes 3145728 | tf_op jit(solution)/shard_map/all_to_all | solution.py:117
  169.0 7.6 %copy-start.13 = (bf16[768,256]{1,0:T(8,128)(2,1)S(1)}, bf16[768,256]{1,0:T(8,128)(2,1)}, u32[]{:S(2)}) copy-start(bf16[768,256]{1,0:T(8,128)(2,1)} %copy-done.12) | copy-start | bytes 1179652
  169.0 13.7 %slice-start = ((s8[6291456]{0:T(1024)(128)(4,1)}), s8[4194304]{0:T(1024)(128)(4,1)S(1)}, s32[]{:S(2)}) async-start(s8[6291456]{0:T(1024)(128)(4,1)} %bitcast.96), calls=%async_computation.11 | async-start | bytes 8388608
  176.6 6.1 %slice-start.1 = ((s8[6291456]{0:T(1024)(128)(4,1)}), s8[2097152]{0:T(1024)(128)(4,1)S(1)}, s32[]{:S(2)}) async-start(s8[6291456]{0:T(1024)(128)(4,1)} %bitcast.96), calls=%async_computation.12 | async-start | bytes 4194304
  176.6 6.1 %copy-start.20 = (f32[768,256]{1,0:T(8,128)S(1)}, f32[768,256]{1,0:T(8,128)}, u32[]{:S(2)}) copy-start(f32[768,256]{1,0:T(8,128)} %fusion) | copy-start | bytes 2359300
  176.7 6.1 %copy-start.21 = (f32[768,256]{1,0:T(8,128)S(1)}, f32[768,256]{1,0:T(8,128)}, u32[]{:S(2)}) copy-start(f32[768,256]{1,0:T(8,128)} %fusion.2) | copy-start | bytes 2359300
  206.5 23.1 %copy-start.4 = (bf16[8,192,512]{2,1,0:T(8,128)(2,1)}, bf16[8,192,512]{2,1,0:T(8,128)(2,1)S(1)}, u32[]{:S(2)}) copy-start(bf16[8,192,512]{2,1,0:T(8,128)(2,1)S(1)} %all-to-all-done.2) | copy-start | bytes 4718596
  220.2 42.5 %all-to-all-start.3 = ((bf16[8,96,1024]{2,1,0:T(8,128)(2,1)}), bf16[8,96,1024]{2,1,0:T(8,128)(2,1)}, u32[]{:S(2)}, u32[]{:S(2)}) async-start(bf16[8,96,1024]{2,1,0:T(8,128)(2,1)} %bitcast.85), calls=%async_computation.4 | async-start | bytes 3145728 | tf_op jit(solution)/shard_map/all_to_all | solution.py:117
  225.8 57.6 %all-gather.11.cloned.1.call-start = ((), (), s32[]{:S(2)}) async-start(), calls=%async_computation.10 | async-start | bytes 1966080 | tf_op jit(solution)/shard_map/all_gather | solution.py:165
  265.4 39.2 %all-gather.9.cloned.1.call-start = ((), (), s32[]{:S(2)}) async-start(), calls=%async_computation.9 | async-start | bytes 1966080 | tf_op jit(solution)/shard_map/all_gather | solution.py:167
  282.4 6.6 %copy-start.17 = (f32[3,512]{1,0:T(4,128)S(1)}, f32[3,512]{1,0:T(4,128)}, u32[]{:S(2)}) copy-start(f32[3,512]{1,0:T(4,128)} %param.21) | copy-start | bytes 18436
  282.4 10.8 %copy-start.14 = (bf16[192,512]{1,0:T(8,128)(2,1)S(1)}, bf16[192,512]{1,0:T(8,128)(2,1)}, u32[]{:S(2)}) copy-start(bf16[192,512]{1,0:T(8,128)(2,1)} %param.17) | copy-start | bytes 589828
  282.4 11.6 %copy-start.15 = (bf16[192,512]{1,0:T(8,128)(2,1)S(1)}, bf16[192,512]{1,0:T(8,128)(2,1)}, u32[]{:S(2)}) copy-start(bf16[192,512]{1,0:T(8,128)(2,1)} %param.18) | copy-start | bytes 589828
  287.7 5.5 %collective-permute-start = (f32[2,512]{1,0:T(2,128)S(1)}, f32[2,512]{1,0:T(2,128)S(1)}, u32[]{:S(2)}, u32[]{:S(2)}) collective-permute-start(f32[2,512]{1,0:T(2,128)S(1)} %slice.24), channel_id=1, source_target_pairs={{4,0},{8,4},{12,8},{16,12},{20,16},{24,20},{28,24},{5,1},{9,5},{13... | collective-permute-start | bytes 12296 | tf_op jit(solution)/shard_map/ppermute | solution.py:12
  304.6 4.0 %copy-start.1 = (bf16[1,256,4096]{2,1,0:T(8,128)(2,1)S(1)}, bf16[1,256,4096]{2,1,0:T(8,128)(2,1)}, u32[]{:S(2)}) copy-start(bf16[1,256,4096]{2,1,0:T(8,128)(2,1)} %param.25) | copy-start | bytes 6291460
  (2 other events, 2.5 us)
Sparse Core Ops, SparseCore 0:
  57.1 45.3 all-gather.4
  104.1 46.3 all-gather.6
  162.3 57.8 reduce-scatter.1
  265.6 17.7 all-gather.10
  284.8 19.8 all-gather.8
where the time goes:
time: 316 us; the launch traced here: 315 us
  waiting for transfers between devices  184 us (58%)
  matrix products  54.2 us (17%)
  starting transfers between devices  24.6 us (8%)
  local copies, waits for them, and re-layouts  18.8 us (6%)
  blocking collectives  15.8 us (5%)
  between operations  14.1 us (4%)
  other arithmetic  3.42 us (1%)
    all_to_all x4, waiting for transfers between devices, over_sp(): return lax.all_to_all(value, 'sp', split_axis=0, concat_axis=0, tiled=True)  112 us
    all_gather x1, waiting for transfers between devices, per_device(): lax.all_gather(part_scaled, 'tp', axis=2, tiled=True)  39 us
    all_to_all x4, starting transfers between devices, over_sp(): return lax.all_to_all(value, 'sp', split_axis=0, concat_axis=0, tiled=True)  22.9 us
    all_to_all x1, blocking collectives, over_sp(): return lax.all_to_all(value, 'sp', split_axis=0, concat_axis=0, tiled=True)  15.8 us
    reduce_scatter x1, waiting for transfers between devices, per_device(): lax.psum_scatter(row_part, 'tp', scatter_dimension=1, tiled=True)  13.8 us
    all_gather x1, waiting for transfers between devices, per_device(): resid_cols = lax.all_gather(own, 'tp', axis=2, tiled=True)  9.86 us
    dot_general x1, matrix products, expert_backward(): lax.dot_general(input_rows, grad_gate, (((0,), (0,)), ((), ())), preferre...  7.59 us
    transpose x3, local copies, waits for them, and re-layouts, by_piece(): return jnp.swapaxes(value, axis, axis + 1).reshape(before + (-1,) + after)  7.21 us
  transfers between devices with their start and end apart: 10, of which 10 were waited for; matrix products, arithmetic and copies ran while one was open for 16% of the time, Pallas kernels for 0%

commit v1 on v0

v1 whole, which is shorter than its diff:
```python
import functools

import jax
import jax.numpy as jnp
from jax import lax
from jax.experimental import pallas as pl
from jax.experimental.pallas import tpu as pltpu
from jax.sharding import PartitionSpec as P

MESH = pl.DeviceIdType.MESH
NN = (((1,), (0,)), ((), ()))
NT = (((1,), (1,)), ((), ()))
TN = (((0,), (0,)), ((), ()))


def dot(a, b, dims=NN):
    return lax.dot_general(a, b, dims, preferred_element_type=jnp.float32)


def each(low, high, step):
    def body(i, carry):
        step(i)
        return carry

    lax.fori_loop(low, high, body, 0)


def spot():
    s, t = lax.axis_index("sp"), lax.axis_index("tp")
    return s, t, lax.div(t, 2), lax.rem(t, 2)


def greet(S, TH):
    s, t, th, tl = spot()
    barrier = pltpu.get_barrier_semaphore()

    def hello(device):
        pl.semaphore_signal(barrier, inc=1, device_id=device, device_id_type=MESH)

    each(1, S, lambda k: hello((lax.rem(s + k, S), t)))
    hello((s, 2 * th + 1 - tl))
    for j in range(1, TH):
        hello((s, 2 * lax.rem(th + j, TH) + tl))
    pl.semaphore_wait(barrier, S - 1 + TH)


def expert_kernel(
    S, T, inp, cot, placed, slot_w, wg_h, wu_h, wd_h,
    back, gwg_h, gwu_h, gwd_h,
    rows, stage, wgu, wd, proj, hid, ggu, part, matebuf, xsend, xrecv, rstage, gout, gdown,
    wsem, gsem, ds, dr, m1s, m1r, xs, xr, m2s, m2r, r1s, r1r, r2s, r2r, rts, rtr,
):
    TH = T // 2
    cap, Q = rows.shape[3], rows.shape[4]
    D = T * Q
    H = wd.shape[0]
    piece = Q // S
    group = D // S
    s, t, th, tl = spot()
    mate = 2 * th + 1 - tl
    source = (inp, cot)

    def other(j):
        return lax.rem(th + j, TH)

    def behind(j):
        return lax.rem(th - j + TH, TH)

    def src_of(k):
        return lax.rem(s - k + S, S)

    weights = [
        pltpu.make_async_copy(wg_h, wgu.at[:, pl.ds(0, H)], wsem.at[0]),
        pltpu.make_async_copy(wu_h, wgu.at[:, pl.ds(H, H)], wsem.at[1]),
        pltpu.make_async_copy(wd_h, wd, wsem.at[2]),
    ]
    for copy in weights:
        copy.start()
    greet(S, TH)

    def remote(src, dst, send, recv, device):
        return pltpu.make_async_remote_copy(
            src_ref=src, dst_ref=dst, send_sem=send, recv_sem=recv, device_id=device, device_id_type=MESH
        )

    def direct(a, k):
        return remote(stage.at[a, k], rows.at[a, s, t], ds.at[a, k], dr.at[a, k], (lax.rem(s + k, S), t))

    def to_mate(a, k):
        block = rows.at[a, src_of(k), t]
        return remote(block, block, m1s.at[a, k], m1r.at[a, k], (s, mate))

    def across(a, j, k):
        block = rows.at[a, src_of(k), t]
        return remote(block, block, xs.at[a, j, k], xr.at[a, j, k], (s, 2 * other(j) + tl))

    def on_to_mate(a, j, k):
        block = rows.at[a, src_of(k), 2 * behind(j) + tl]
        return remote(block, block, m2s.at[a, j, k], m2r.at[a, j, k], (s, mate))

    def pick(a, e, columns):
        picked = dot(placed[e], source[a][:, columns])
        if a == 1:
            picked = picked * slot_w[e]
        return picked.astype(jnp.bfloat16)

    def send(a, k):
        stage[a, k] = pick(a, lax.rem(s + k, S), pl.ds(pl.multiple_of(t * Q, Q), Q))
        direct(a, k).start()

    def own(a):
        for q in range(T):
            rows[a, s, q] = pick(a, s, pl.ds(q * Q, Q))

    def forward(a, k):
        direct(a, k).wait_recv()
        for j in range(1, TH):
            across(a, j, k).start()
        to_mate(a, k).start()

    def forward_on(a, k):
        for j in range(1, TH):
            across(a, j, k).wait_recv()
            on_to_mate(a, j, k).start()

    def complete(a, k):
        to_mate(a, k).wait_recv()
        for j in range(1, TH):
            on_to_mate(a, j, k).wait_recv()

    def project(k):
        b = src_of(k)
        total = dot(rows[0, b, 0], wgu[pl.ds(0, Q), :])
        for q in range(1, T):
            total = total + dot(rows[0, b, q], wgu[pl.ds(q * Q, Q), :])
        proj[b] = total

    def half(k):
        return remote(
            part.at[lax.rem(k, 2), 1 - tl], matebuf.at[k], r1s.at[k], r1r.at[k], (s, mate)
        )

    def chip_sum(j, k):
        return remote(xsend.at[j, k], xrecv.at[j, k], r2s.at[j, k], r2r.at[j, k], (s, 2 * other(j) + tl))

    def give_back(k):
        return remote(rstage.at[k], back.at[s], rts.at[k], rtr.at[k], (src_of(k), t))

    def gradients(k):
        b = src_of(k)
        grad_hidden = dot(rows[1, b, 0], wd[:, pl.ds(0, Q)], NT)
        for q in range(1, T):
            grad_hidden = grad_hidden + dot(rows[1, b, q], wd[:, pl.ds(q * Q, Q)], NT)
        gate, up = proj[b][:, :H], proj[b][:, H:]
        sig = jax.nn.sigmoid(gate)
        act = gate * sig
        slope = sig * (1.0 + gate * (1.0 - sig))
        hid[b] = (act * up).astype(jnp.bfloat16)
        ggu[b, :, pl.ds(0, H)] = (grad_hidden * up * slope).astype(jnp.bfloat16)
        ggu[b, :, pl.ds(H, H)] = (grad_hidden * act).astype(jnp.bfloat16)

        @pl.when(k >= 2)
        def _():
            half(k - 2).wait_send()

        slot = lax.rem(k, 2)
        grads = ggu[b]
        for g in range(S):
            some = dot(grads, wgu[pl.ds(g * group, group), :], NT)
            for q in range(T):
                part[slot, q % 2, q // 2, :, pl.ds(g * piece, piece)] = some[:, q * piece : (q + 1) * piece]
        half(k).start()

    def reduce_chip(k):
        half(k).wait_recv()
        slot = lax.rem(k, 2)
        for j in range(1, TH):
            o = other(j)
            xsend[j, k] = (part[slot, tl, o] + matebuf[k, o]).astype(jnp.bfloat16)
            chip_sum(j, k).start()
        matebuf[k, th] = part[slot, tl, th] + matebuf[k, th]

    def reduce_all(k):
        total = matebuf[k, th]
        for j in range(1, TH):
            chip_sum(j, k).wait_recv()
            total = total + xrecv[j, k].astype(jnp.float32)
        rstage[k] = total.astype(jnp.bfloat16)

        @pl.when(k >= 1)
        def _():
            give_back(k).start()

    keep = pltpu.make_async_copy(rstage.at[0], back.at[s], rts.at[0])

    each(1, S, lambda k: send(0, k))
    own(0)
    each(1, S, lambda k: send(1, k))
    own(1)
    for copy in weights:
        copy.wait()
    project(0)

    def first(i):
        @pl.when(i < S)
        def _():
            forward(0, i)

        @pl.when((i >= 2) & (i < S + 1))
        def _():
            forward_on(0, i - 1)

        @pl.when(i >= 3)
        def _():
            complete(0, i - 2)
            project(i - 2)

    each(1, S + 2, first)
    gradients(0)

    def second(i):
        @pl.when(i < S)
        def _():
            forward(1, i)

        @pl.when((i >= 2) & (i < S + 1))
        def _():
            forward_on(1, i - 1)

        @pl.when((i >= 3) & (i < S + 3))
        def _():
            reduce_chip(i - 3)

        @pl.when((i >= 3) & (i < S + 2))
        def _():
            complete(1, i - 2)
            gradients(i - 2)

        @pl.when(i >= 4)
        def _():
            reduce_all(i - 4)

    each(1, S + 4, second)
    keep.start()

    tile = min(512, Q)
    per = Q // tile

    def weight_grads(i):
        q, c = lax.div(i, per), pl.multiple_of(lax.rem(i, per) * tile, tile)
        x = rows[0, :, q, :, pl.ds(c, tile)].reshape(S * cap, tile)
        start = pl.multiple_of(q * Q + c, tile)
        gout[pl.ds(start, tile), :] = dot(x, ggu[...].reshape(S * cap, 2 * H), TN).astype(jnp.bfloat16)
        d = rows[1, :, q, :, pl.ds(c, tile)].reshape(S * cap, tile)
        gdown[:, pl.ds(start, tile)] = dot(hid[...].reshape(S * cap, H), d, TN).astype(jnp.bfloat16)

    each(0, T * per, weight_grads)
    results = [
        pltpu.make_async_copy(gout.at[:, pl.ds(0, H)], gwg_h, gsem.at[0]),
        pltpu.make_async_copy(gout.at[:, pl.ds(H, H)], gwu_h, gsem.at[1]),
        pltpu.make_async_copy(gdown, gwd_h, gsem.at[2]),
    ]
    for copy in results:
        copy.start()

    half(S - 2).wait_send()
    half(S - 1).wait_send()

    def finish(k):
        for a in range(2):
            direct(a, k).wait_send()
            to_mate(a, k).wait_send()
            for j in range(1, TH):
                across(a, j, k).wait_send()
                on_to_mate(a, j, k).wait_send()
        give_back(k).wait_send()
        give_back(k).wait_recv()

    each(1, S, finish)

    def finish_sums(k):
        for j in range(1, TH):
            chip_sum(j, k).wait_send()

    each(0, S, finish_sums)
    keep.wait()
    for copy in results:
        copy.wait()


def expert_exchange(S, T, cap, inp, cot, placed, slot_w, w_gate, w_up, w_down):
    tok, D = inp.shape
    H = w_down.shape[0]
    TH, Q = T // 2, D // T
    bf, f32 = jnp.bfloat16, jnp.float32
    dma = pltpu.SemaphoreType.DMA
    vmem = pl.BlockSpec(memory_space=pltpu.VMEM)
    hbm = pl.BlockSpec(memory_space=pl.ANY)
    rows = S * cap
    return pl.pallas_call(
        functools.partial(expert_kernel, S, T),
        name="expert_exchange",
        out_shape=(
            jax.ShapeDtypeStruct((S, cap, Q), bf),
            jax.ShapeDtypeStruct((D, H), bf),
            jax.ShapeDtypeStruct((D, H), bf),
            jax.ShapeDtypeStruct((H, D), bf),
        ),
        in_specs=[vmem] * 4 + [hbm] * 3,
        out_specs=(hbm,) * 4,
        scratch_shapes=[
            pltpu.VMEM((2, S, T, cap, Q), bf),
            pltpu.VMEM((2, S, cap, Q), bf),
            pltpu.VMEM((D, 2 * H), bf),
            pltpu.VMEM((H, D), bf),
            pltpu.VMEM((S, cap, 2 * H), f32),
            pltpu.VMEM((S, cap, H), bf),
            pltpu.VMEM((S, cap, 2 * H), bf),
            pltpu.VMEM((2, 2, TH, cap, Q), f32),
            pltpu.VMEM((S, TH, cap, Q), f32),
            pltpu.VMEM((TH, S, cap, Q), bf),
            pltpu.VMEM((TH, S, cap, Q), bf),
            pltpu.VMEM((S, cap, Q), bf),
            pltpu.VMEM((D, 2 * H), bf),
            pltpu.VMEM((H, D), bf),
            dma((3,)), dma((3,)),
            dma((2, S)), dma((2, S)),
            dma((2, S)), dma((2, S)),
            dma((2, TH, S)), dma((2, TH, S)),
            dma((2, TH, S)), dma((2, TH, S)),
            dma((S,)), dma((S,)),
            dma((TH, S)), dma((TH, S)),
            dma((S,)), dma((S,)),
        ],
        cost_estimate=pl.CostEstimate(
            flops=16 * rows * D * H, bytes_accessed=8 * rows * D + 24 * D * H, transcendentals=rows * H
        ),
        compiler_params=pltpu.CompilerParams(
            collective_id=0, has_side_effects=True, vmem_limit_bytes=67_043_328
        ),
    )(inp, cot, placed, slot_w, w_gate, w_up, w_down)


def slot_masks(routes, route_weight, experts, capacity):
    tok_rows = routes.shape[0]
    names = jnp.arange(experts, dtype=jnp.int32)
    hits = routes[None, :, :] == names[:, None, None]
    chosen = jnp.any(hits, axis=2)
    weight = jnp.sum(jnp.where(hits, route_weight[None], 0.0), axis=2)
    order = jnp.arange(tok_rows, dtype=jnp.int32)
    before = (order[:, None] < order[None, :]).astype(jnp.bfloat16)
    rank = jnp.dot(chosen.astype(jnp.bfloat16), before, preferred_element_type=jnp.float32)
    rank = jnp.where(chosen, rank.astype(jnp.int32), -1)
    slots = jnp.arange(capacity, dtype=jnp.int32)
    placed = rank[:, None, :] == slots[None, :, None]
    slot_weight = jnp.sum(jnp.where(placed, weight[:, None, :], 0.0), axis=2, keepdims=True)
    return placed.astype(jnp.bfloat16), slot_weight


def from_behind(value, axis, steps):
    count = lax.axis_size(axis)
    leading, last = (max(0, -steps), min(count, count - steps))
    return lax.ppermute(value, axis, [(source, source + steps) for source in range(leading, last)])


def per_device(
    cotangent, moe_input, routes, route_weight, conv_input, input_gate, output_gate, conv_output,
    taps, w_out, w_gate, w_up, w_down,
):
    experts = lax.axis_size("sp")
    tp_size = lax.axis_size("tp")
    tok_rows, top_k = routes.shape
    model_width = cotangent.shape[1]
    capacity = -(-max(2, 2 * tok_rows * top_k // experts) // 16) * 16
    part_width = model_width // tp_size
    piece = part_width // experts
    tp_index = lax.axis_index("tp")
    placed, slot_weight = slot_masks(routes, route_weight, experts, capacity)
    returned, gate_wgrad, up_wgrad, grad_down = expert_exchange(
        experts, tp_size, capacity, moe_input, cotangent, placed, slot_weight, w_gate[0], w_up[0], w_down[0]
    )
    mixed = (output_gate.astype(jnp.float32) * conv_output.astype(jnp.float32)).astype(jnp.bfloat16)

    def over_sp(value):
        return lax.all_to_all(value, "sp", split_axis=0, concat_axis=0, tiled=True)

    out_turned = w_out.reshape(experts, tp_size, piece, -1).swapaxes(0, 1).reshape(model_width, -1)
    cot_share = cotangent.reshape(tok_rows, experts, tp_size, piece)
    cot_share = lax.dynamic_index_in_dim(cot_share, tp_index, 2, keepdims=False)
    cot_share = cot_share.reshape(tok_rows, part_width)
    mixed_all = over_sp(jnp.broadcast_to(mixed[None], (experts,) + mixed.shape))
    mixed_all = mixed_all.reshape(experts * tok_rows, -1)
    route_sum = cot_share.astype(jnp.float32) + lax.dot_general(
        placed.reshape(experts * capacity, tok_rows),
        returned.reshape(experts * capacity, part_width),
        (((0,), (0,)), ((), ())),
        preferred_element_type=jnp.float32,
    )
    resid_part = route_sum.astype(jnp.bfloat16)
    resid_grad = lax.all_gather(resid_part, "tp", axis=1, tiled=True)
    own = over_sp(jnp.swapaxes(resid_part.reshape(tok_rows, experts, piece), 0, 1))
    resid_cols = lax.all_gather(own, "tp", axis=2, tiled=True)
    resid_cols = resid_cols.reshape(experts * tok_rows, model_width // experts)
    grad_w_out = lax.dot_general(
        resid_cols, mixed_all, (((0,), (0,)), ((), ())), preferred_element_type=jnp.float32
    )
    grad_mixed = jnp.dot(resid_grad, out_turned, preferred_element_type=jnp.float32)
    grad_output_gate = (grad_mixed * conv_output.astype(jnp.float32)).astype(jnp.bfloat16)
    grad_conv = grad_mixed * output_gate.astype(jnp.float32)
    following = from_behind(grad_conv[:2], "sp", -1)
    extended = jnp.concatenate([grad_conv, following], axis=0)
    grad_g = (
        taps[2] * extended[:tok_rows]
        + taps[1] * extended[1 : tok_rows + 1]
        + taps[0] * extended[2:]
    )
    grad_conv_input = (grad_g * input_gate.astype(jnp.float32)).astype(jnp.bfloat16)
    grad_input_gate = (grad_g * conv_input.astype(jnp.float32)).astype(jnp.bfloat16)
    return (
        gate_wgrad[None], up_wgrad[None], grad_down[None], grad_w_out,
        grad_conv_input, grad_input_gate, grad_output_gate,
    )


def solution(mesh):
    return jax.shard_map(
        per_device,
        mesh=mesh,
        in_specs=(
            P("sp", None), P("sp", None), P("sp", None), P("sp", None),
            P("sp", "tp"), P("sp", "tp"), P("sp", "tp"), P("sp", "tp"),
            P(None, "tp"), P(None, "tp"),
            P("sp", None, "tp"), P("sp", None, "tp"), P("sp", "tp", None),
        ),
        out_specs=(
            P("sp", None, "tp"), P("sp", None, "tp"), P("sp", "tp", None),
            P("sp", "tp"), P("sp", "tp"), P("sp", "tp"), P("sp", "tp"),
        ),
        check_vma=False,
    )
```

time: 316 us -> 261 us (0.83)
  Pallas kernels: 0 us -> 157 us
  waiting for transfers between devices: 184 us -> 42.6 us
  matrix products: 54.2 us -> 10.9 us
  blocking collectives: 15.8 us -> 0 us
  starting transfers between devices: 24.6 us -> 12.1 us
    pallas_call x0 -> x1, Pallas kernels: none -> 157 us  [expert_exchange(): pl.pallas_call(functools.partial(expert_kernel, S, T), name='expert_excha...]
    all_to_all x4 -> x2, waiting for transfers between devices: 112 us -> 14.2 us  [over_sp(): return lax.all_to_all(value, 'sp', split_axis=0, concat_axis=0, tiled=True)]
    all_gather x2 -> x0, waiting for transfers between devices: 43.2 us -> none  [the longest x1 39 us: per_device(): lax.all_gather(part_scaled, 'tp', axis=2, tiled=True)]
    dot_general x11 -> x1, matrix products: 45.7 us -> 2.92 us  [per_device(): lax.dot_general(placed.reshape(experts * capacity, tok_rows), returned.re...]
    all_to_all x1 -> x0, blocking collectives: 15.8 us -> none  [over_sp(): return lax.all_to_all(value, 'sp', split_axis=0, concat_axis=0, tiled=True)]
    reduce_scatter x1 -> x0, waiting for transfers between devices: 13.8 us -> none  [per_device(): lax.psum_scatter(row_part, 'tp', scatter_dimension=1, tiled=True)]
    all_to_all x4 -> x2, starting transfers between devices: 22.9 us -> 10.8 us  [over_sp(): return lax.all_to_all(value, 'sp', split_axis=0, concat_axis=0, tiled=True)]
    all_gather x1, waiting for transfers between devices: 0.96 us -> 8.06 us  [per_device(): resid_grad = lax.all_gather(resid_part, 'tp', axis=1, tiled=True)]
  transfers between devices with their start and end apart: 10 -> 5, of which waited for: 10 -> 4; matrix products, arithmetic and copies ran while one was open for 16% -> 5% of each run, Pallas kernels for 0% -> 0%
where the time goes in v1:
time: 261 us; the launch traced here: 260 us
  Pallas kernels  157 us (60%)
  waiting for transfers between devices  42.6 us (16%)
  local copies, waits for them, and re-layouts  18.6 us (7%)
  between operations  14.1 us (5%)
  starting transfers between devices  12.1 us (5%)
  matrix products  10.9 us (4%)
  other arithmetic  4.95 us (2%)
    pallas_call x1, Pallas kernels, expert_exchange(): pl.pallas_call(functools.partial(expert_kernel, S, T), name='expert_excha...  157 us
    all_to_all x2, waiting for transfers between devices, over_sp(): return lax.all_to_all(value, 'sp', split_axis=0, concat_axis=0, tiled=True)  14.2 us
    all_gather x1, waiting for transfers between devices, per_device(): resid_cols = lax.all_gather(own, 'tp', axis=2, tiled=True)  13.5 us
    all_to_all x2, starting transfers between devices, over_sp(): return lax.all_to_all(value, 'sp', split_axis=0, concat_axis=0, tiled=True)  10.8 us
    all_gather x1, waiting for transfers between devices, per_device(): resid_grad = lax.all_gather(resid_part, 'tp', axis=1, tiled=True)  8.06 us
    ppermute x1, waiting for transfers between devices, from_behind(): lax.ppermute(value, axis, [(source, source + steps) for source in range(l...  6.13 us
    unnamed x23, local copies, waits for them, and re-layouts  6.04 us
  transfers between devices with their start and end apart: 5, of which 4 were waited for; matrix products, arithmetic and copies ran while one was open for 5% of the time, Pallas kernels for 0%

profile of v1, /device:TPU:0, one launch (start us, length us, event | category | flops | bytes accessed | tf_op | source)
XLA Modules:
  0.0 260.2 jit_solution(13430123027657758309)
XLA Ops:
  7.2 0.7 fusion.12
  7.9 0.1 fusion.2
  8.1 0.7 select_reduce_fusion.1
  8.8 0.8 fusion.3.placed
  9.6 0.2 select_reduce_fusion
  9.8 0.9 copy.38.slot_w
  10.8 2.8 %reshape.39 = bf16[192,8,4,128]{3,2,1,0:T(4,128)(2,1)S(1)} reshape(bf16[192,4096]{1,0:T(8,128)(2,1)} %cot.1) | data formatting | bytes 3145728 | tf_op jit(solution)/shard_map/reshape | solution.py:388
  13.6 0.8 constant_dynamic-slice_fusion
  14.4 0.9 copy_convert_fusion
  15.4 156.9 %expert_exchange.1 = (bf16[8,96,1024]{2,1,0:T(8,128)(2,1)}, bf16[4096,256]{1,0:T(8,128)(2,1)}, bf16[4096,256]{1,0:T(8,128)(2,1)}, bf16[256,4096]{1,0:T(8,128)(2,1)}) custom-call(bf16[192,4096]{1,0:T(8,128)(2,1)} %inp.1, bf16[192,4096]{1,0:T(8,128)(2,1)} %cot.1, bf16[8,96,192]{2,1,0:T(8,128)(2,1)} %fusion.3.placed, f32[8,96,1]{2,1,0:T(8,128)} %copy.38.slot_w, ...), custom_call_target="tpu_custom_call" | custom-call | flops 12884901888 | bytes 50331648 | tf_op jit(solution)/shard_map/expert_exchange/pallas_call | solution.py:300
  172.2 2.9 %fusion.1 = bf16[192,1024]{1,0:T(8,128)(2,1)} fusion(bf16[8,96,1024]{2,1,0:T(8,128)(2,1)} %get-tuple-element.14, f32[24,8,8,128]{3,2,1,0:T(8,128)} %bitcast.45, s32[8,192]{1,0:T(8,128)} %copy-done.8), kind=kOutput, calls=%fused_computation.3 | convolution fusion | flops 302530560 | bytes 2758656 | tf_op jit(solution)/shard_map/dot_general | solution.py:393
  175.2 1.8 bitcast_bitcast_fusion
  177.0 5.1 %all-to-all-start = ((bf16[8,192,128]{2,1,0:T(8,128)(2,1)}), bf16[8,192,128]{2,1,0:T(8,128)(2,1)S(1)}, u32[]{:S(2)}, u32[]{:S(2)}) async-start(bf16[8,192,128]{2,1,0:T(8,128)(2,1)} %bitcast_bitcast_fusion), calls=%async_computation | async-start | bytes 786432 | tf_op jit(solution)/shard_map/all_to_all | solution.py:385
  182.1 4.9 %copy.42 = bf16[4,8,128,512]{3,2,1,0:T(8,128)(2,1)} copy(bf16[4,8,128,512]{3,2,0,1:T(8,128)(2,1)} %bitcast.41) | data formatting | bytes 8388608 | tf_op jit(solution)/shard_map/transpose | solution.py:387
  187.0 8.1 %all-gather.5.cloned.1.call-done = bf16[192,4096]{1,0:T(8,128)(2,1)} async-done(((bf16[192,1024]{1,0:T(8,128)(2,1)}), bf16[192,4096]{1,0:T(8,128)(2,1)}) %all-gather.5.cloned.1.call-update) | async-done | bytes 1572880 | tf_op jit(solution)/shard_map/all_gather | solution.py:400
  195.1 4.3 %fusion.9 = (bf16[192,512]{1,0:T(8,128)(2,1)}, f32[192,512]{1,0:T(8,128)S(1)}, bf16[192,512]{1,0:T(8,128)(2,1)S(1)}) fusion(bf16[192,512]{1,0:T(8,128)(2,1)S(1)} %copy-done.6, bf16[192,512]{1,0:T(8,128)(2,1)S(1)} %copy-done.7, bf16[192,4096]{1,0:T(8,128)(2,1)} %all-gather.5.cloned.1.call-done, bf16[4096,512]{1,0:T(8,128)(2,1)} %bitcast.40), kind=kOutput, calls=%fused_computation.19 | convolution fusion | flops 805994496 | bytes 6946816 | tf_op jit(solution)/shard_map/dot_general | solution.py:407
  199.5 1.3 broadcast_in_dim.63
  200.7 5.6 %all-to-all-start.1 = ((bf16[8,192,512]{2,1,0:T(8,128)(2,1)}), bf16[8,192,512]{2,1,0:T(8,128)(2,1)S(1)}, u32[]{:S(2)}, u32[]{:S(2)}) async-start(bf16[8,192,512]{2,1,0:T(8,128)(2,1)} %broadcast_in_dim.63), calls=%async_computation.1 | async-start | bytes 3145728 | tf_op jit(solution)/shard_map/all_to_all | solution.py:385
  206.4 0.0 all-gather.3.cloned.1.call-start
  206.4 0.7 all-gather.3.cloned.1.call-update
  207.2 1.3 collective-permute-start
  208.5 6.1 %collective-permute-done = f32[2,512]{1,0:T(2,128)S(1)} collective-permute-done((f32[2,512]{1,0:T(2,128)S(1)}, f32[2,512]{1,0:T(2,128)S(1)}, u32[]{:S(2)}, u32[]{:S(2)}) %collective-permute-start) | collective-permute-done | bytes 4128 | tf_op jit(solution)/shard_map/ppermute | solution.py:363
  214.6 0.8 multiply_convert_fusion
  215.4 0.7 multiply_convert_fusion.1
  216.2 13.5 %all-gather.3.cloned.1.call-done = bf16[8,192,512]{2,1,0:T(8,128)(2,1)} async-done(((bf16[8,192,128]{2,1,0:T(8,128)(2,1)}), bf16[8,192,512]{2,1,0:T(8,128)(2,1)}) %all-gather.3.cloned.1.call-update) | async-done | bytes 1572880 | tf_op jit(solution)/shard_map/all_gather | solution.py:402
  229.6 14.2 %all-to-all-done.1 = bf16[8,192,512]{2,1,0:T(8,128)(2,1)S(1)} async-done(((bf16[8,192,512]{2,1,0:T(8,128)(2,1)}), bf16[8,192,512]{2,1,0:T(8,128)(2,1)S(1)}, u32[]{:S(2)}, u32[]{:S(2)}) %all-to-all-start.1) | async-done | bytes 1572896 | tf_op jit(solution)/shard_map/all_to_all | solution.py:385
  243.8 3.5 %convolution_bitcast_fusion = f32[512,512]{1,0:T(8,128)} fusion(bf16[8,192,512]{2,1,0:T(8,128)(2,1)} %all-gather.3.cloned.1.call-done, bf16[8,192,512]{2,1,0:T(8,128)(2,1)S(1)} %all-to-all-done.1), kind=kOutput, calls=%fused_computation | convolution fusion | flops 805306368 | bytes 4194304 | tf_op jit(solution)/shard_map/dot_general | solution.py:404
  247.4 1.3 copy.53
  248.7 1.0 copy-done.1
  249.7 1.3 copy.54
  251.0 1.0 copy-done
  252.1 1.3 copy.55
  (23 shorter events, 0.1 us)
Async XLA Ops:
  7.2 187.9 %all-gather.5.cloned.1.call-start = ((), (), s32[]{:S(2)}) async-start(), calls=%async_computation.3 | async-start | bytes 1966080 | tf_op jit(solution)/shard_map/all_gather | solution.py:400
  8.1 1.6 copy-start.8
  177.0 22.4 %all-to-all-start = ((bf16[8,192,128]{2,1,0:T(8,128)(2,1)}), bf16[8,192,128]{2,1,0:T(8,128)(2,1)S(1)}, u32[]{:S(2)}, u32[]{:S(2)}) async-start(bf16[8,192,128]{2,1,0:T(8,128)(2,1)} %bitcast_bitcast_fusion), calls=%async_computation | async-start | bytes 786432 | tf_op jit(solution)/shard_map/all_to_all | solution.py:385
  182.1 13.0 %copy-start.6 = (bf16[192,512]{1,0:T(8,128)(2,1)S(1)}, bf16[192,512]{1,0:T(8,128)(2,1)}, u32[]{:S(2)}) copy-start(bf16[192,512]{1,0:T(8,128)(2,1)} %param.20) | copy-start | bytes 589828
  182.1 13.0 %copy-start.7 = (bf16[192,512]{1,0:T(8,128)(2,1)S(1)}, bf16[192,512]{1,0:T(8,128)(2,1)}, u32[]{:S(2)}) copy-start(bf16[192,512]{1,0:T(8,128)(2,1)} %param.19) | copy-start | bytes 589828
  199.4 1.3 copy-start.3
  200.7 7.7 %copy-start.9 = (f32[3,512]{1,0:T(4,128)S(1)}, f32[3,512]{1,0:T(4,128)}, u32[]{:S(2)}) copy-start(f32[3,512]{1,0:T(4,128)} %param.21) | copy-start | bytes 18436
  200.7 13.9 %copy-start.4 = (bf16[192,512]{1,0:T(8,128)(2,1)S(1)}, bf16[192,512]{1,0:T(8,128)(2,1)}, u32[]{:S(2)}) copy-start(bf16[192,512]{1,0:T(8,128)(2,1)} %param.17) | copy-start | bytes 589828
  200.7 43.1 %all-to-all-start.1 = ((bf16[8,192,512]{2,1,0:T(8,128)(2,1)}), bf16[8,192,512]{2,1,0:T(8,128)(2,1)S(1)}, u32[]{:S(2)}, u32[]{:S(2)}) async-start(bf16[8,192,512]{2,1,0:T(8,128)(2,1)} %broadcast_in_dim.63), calls=%async_computation.1 | async-start | bytes 3145728 | tf_op jit(solution)/shard_map/all_to_all | solution.py:385
  206.4 9.1 %copy-start.5 = (bf16[192,512]{1,0:T(8,128)(2,1)S(1)}, bf16[192,512]{1,0:T(8,128)(2,1)}, u32[]{:S(2)}) copy-start(bf16[192,512]{1,0:T(8,128)(2,1)} %param.18) | copy-start | bytes 589828
  206.4 23.3 %all-gather.3.cloned.1.call-start = ((), (), s32[]{:S(2)}) async-start(), calls=%async_computation.2 | async-start | bytes 1966080 | tf_op jit(solution)/shard_map/all_gather | solution.py:402
  207.2 7.5 %collective-permute-start = (f32[2,512]{1,0:T(2,128)S(1)}, f32[2,512]{1,0:T(2,128)S(1)}, u32[]{:S(2)}, u32[]{:S(2)}) collective-permute-start(f32[2,512]{1,0:T(2,128)S(1)} %slice.24), channel_id=1, source_target_pairs={{4,0},{8,4},{12,8},{16,12},{20,16},{24,20},{28,24},{5,1},{9,5},{13... | collective-permute-start | bytes 12296 | tf_op jit(solution)/shard_map/ppermute | solution.py:363
  243.8 3.5 %copy-start.2 = (bf16[4096,256]{1,0:T(8,128)(2,1)S(1)}, bf16[4096,256]{1,0:T(8,128)(2,1)}, u32[]{:S(2)}) copy-start(bf16[4096,256]{1,0:T(8,128)(2,1)} %get-tuple-element.11) | copy-start | bytes 6291460
  247.4 2.3 copy-start.1
  249.7 2.3 copy-start
Sparse Core Ops, SparseCore 0:
  175.3 19.7 all-gather.4
  209.3 20.2 all-gather.2

commit v2 on v1

v2 whole, which is shorter than its diff:
```python
import functools

import jax
import jax.numpy as jnp
from jax import lax
from jax.experimental import pallas as pl
from jax.experimental.pallas import tpu as pltpu
from jax.sharding import PartitionSpec as P

NEAR = 2
MESH = pl.DeviceIdType.MESH
NN = (((1,), (0,)), ((), ()))
NT = (((1,), (1,)), ((), ()))
TN = (((0,), (0,)), ((), ()))


def dot(a, b, dims=NN):
    return lax.dot_general(a, b, dims, preferred_element_type=jnp.float32)


def each(low, high, step):
    def body(i, carry):
        step(i)
        return carry

    lax.fori_loop(low, high, body, 0)


def spot():
    s, t = lax.axis_index("sp"), lax.axis_index("tp")
    return s, t, lax.div(t, 2), lax.rem(t, 2)


def flip(S, a, b):
    total, weight = 0, 1
    while weight < S:
        p, q = lax.rem(lax.div(a, weight), 2), lax.rem(lax.div(b, weight), 2)
        total, weight = total + (p + q - 2 * p * q) * weight, 2 * weight
    return total


def partner(S, s, i):
    if S < 4:
        return i
    high, low = lax.div(s, S // 2), lax.rem(lax.div(s, S // 4), 2)
    inner = high + low - 2 * high * low
    turned = S // 2 + lax.rem(i - S // 2 + inner * (S // 4) + S, S // 2)
    return jnp.where(i >= S // 2, turned, i)


def remote(src, dst, send, recv, device):
    return pltpu.make_async_remote_copy(
        src_ref=src, dst_ref=dst, send_sem=send, recv_sem=recv, device_id=device, device_id_type=MESH
    )


def greet(S, TH):
    s, t, th, tl = spot()
    barrier = pltpu.get_barrier_semaphore()

    def hello(device):
        pl.semaphore_signal(barrier, inc=1, device_id=device, device_id_type=MESH)

    each(1, S, lambda k: hello((lax.rem(s + k, S), t)))
    hello((s, 2 * th + 1 - tl))
    for j in range(1, TH):
        hello((s, 2 * lax.rem(th + j, TH) + tl))
    pl.semaphore_wait(barrier, S - 1 + TH)


def expert_kernel(
    S, T, inp, cot, placed, slot_w, out_gate, conv_out, wg_h, wu_h, wd_h,
    back, mix_all, gwg_h, gwu_h, gwd_h,
    mix, rows, stage, wgu, wd, proj, hid, ggu, part, matebuf, total_part, near, xsend, xrecv, rstage, gout, gdown,
    wsem, gsem, ds, dr, m1s, m1r, xs, xr, m2s, m2r, r1s, r1r, r2s, r2r, rts, rtr, us, ur, vs, vr, ys, yr,
):
    TH = T // 2
    cap, Q = rows.shape[3], rows.shape[4]
    D = T * Q
    H = wd.shape[0]
    piece = Q // S
    group = D // S
    s, t, th, tl = spot()
    mate = 2 * th + 1 - tl
    source = (inp, cot)

    def other(j):
        return lax.rem(th + j, TH)

    def behind(j):
        return lax.rem(th - j + TH, TH)

    def src_of(k):
        return flip(S, s, k)

    def at(i):
        return partner(S, s, i)

    weights = [
        pltpu.make_async_copy(wg_h, wgu.at[:, pl.ds(0, H)], wsem.at[0]),
        pltpu.make_async_copy(wu_h, wgu.at[:, pl.ds(H, H)], wsem.at[1]),
        pltpu.make_async_copy(wd_h, wd, wsem.at[2]),
    ]
    for copy in weights:
        copy.start()
    greet(S, TH)

    def direct(a, k):
        return remote(stage.at[a, k], rows.at[a, s, t], ds.at[a, k], dr.at[a, k], (src_of(k), t))

    def direct_too(a, j, k):
        q = 2 * other(j) + tl
        return remote(near.at[a, j, k], rows.at[a, s, q], xs.at[a, j, k], xr.at[a, TH - j, k], (src_of(k), t))

    def to_mate(a, k):
        block = rows.at[a, src_of(k), t]
        return remote(block, block, m1s.at[a, k], m1r.at[a, k], (s, mate))

    def across(a, j, k):
        block = rows.at[a, src_of(k), t]
        return remote(block, block, xs.at[a, j, k], xr.at[a, j, k], (s, 2 * other(j) + tl))

    def on_to_mate(a, j, k):
        block = rows.at[a, src_of(k), 2 * behind(j) + tl]
        return remote(block, block, m2s.at[a, j, k], m2r.at[a, j, k], (s, mate))

    def pick(a, e, columns):
        picked = dot(placed[e], source[a][:, columns])
        if a == 1:
            picked = picked * slot_w[e]
        return picked.astype(jnp.bfloat16)

    def send(a, k):
        stage[a, k] = pick(a, src_of(k), pl.ds(pl.multiple_of(t * Q, Q), Q))
        direct(a, k).start()

        @pl.when(k < NEAR)
        def _():
            for j in range(1, TH):
                near[a, j, k] = pick(a, src_of(k), pl.ds(pl.multiple_of((2 * other(j) + tl) * Q, Q), Q))
                direct_too(a, j, k).start()

    def own(a):
        for q in range(T):
            rows[a, s, q] = pick(a, s, pl.ds(q * Q, Q))

    def forward(a, k):
        direct(a, k).wait_recv()

        @pl.when(k >= NEAR)
        def _():
            for j in range(1, TH):
                across(a, j, k).start()

        to_mate(a, k).start()

    def forward_on(a, k):
        for j in range(1, TH):
            across(a, j, k).wait_recv()
            on_to_mate(a, j, k).start()

    def complete(a, k):
        to_mate(a, k).wait_recv()
        for j in range(1, TH):
            on_to_mate(a, j, k).wait_recv()

    def project(k):
        b = src_of(k)
        total = dot(rows[0, b, 0], wgu[pl.ds(0, Q), :])
        for q in range(1, T):
            total = total + dot(rows[0, b, q], wgu[pl.ds(q * Q, Q), :])
        proj[b] = total

    def half(n):
        return remote(part.at[lax.rem(n, 2), 1 - tl], matebuf.at[n], r1s.at[n], r1r.at[n], (s, mate))

    def chip_sum(j, k):
        return remote(xsend.at[j, k], xrecv.at[j, k], r2s.at[j, k], r2r.at[j, k], (s, 2 * other(j) + tl))

    def give_back(k):
        return remote(rstage.at[k], back.at[s], rts.at[k], rtr.at[k], (src_of(k), t))

    def gradients(n, k):
        b = src_of(k)
        grad_hidden = dot(rows[1, b, 0], wd[:, pl.ds(0, Q)], NT)
        for q in range(1, T):
            grad_hidden = grad_hidden + dot(rows[1, b, q], wd[:, pl.ds(q * Q, Q)], NT)
        gate, up = proj[b][:, :H], proj[b][:, H:]
        sig = jax.nn.sigmoid(gate)
        act = gate * sig
        slope = sig * (1.0 + gate * (1.0 - sig))
        hid[b] = (act * up).astype(jnp.bfloat16)
        ggu[b, :, pl.ds(0, H)] = (grad_hidden * up * slope).astype(jnp.bfloat16)
        ggu[b, :, pl.ds(H, H)] = (grad_hidden * act).astype(jnp.bfloat16)

        @pl.when(n >= 2)
        def _():
            half(n - 2).wait_send()

        slot = lax.rem(n, 2)
        grads = ggu[b]
        for g in range(S):
            some = dot(grads, wgu[pl.ds(g * group, group), :], NT)
            for q in range(T):
                part[slot, q % 2, q // 2, :, pl.ds(g * piece, piece)] = some[:, q * piece : (q + 1) * piece]
        half(n).start()

    def reduce_chip(n, k):
        half(n).wait_recv()
        slot = lax.rem(n, 2)
        for j in range(1, TH):
            o = other(j)
            xsend[j, k] = (part[slot, tl, o] + matebuf[n, o]).astype(jnp.bfloat16)
            chip_sum(j, k).start()
        total_part[slot] = part[slot, tl, th] + matebuf[n, th]

    def reduce_all(n, k):
        total = total_part[lax.rem(n, 2)]
        for j in range(1, TH):
            chip_sum(j, k).wait_recv()
            total = total + xrecv[j, k].astype(jnp.float32)
        rstage[k] = total.astype(jnp.bfloat16)

        @pl.when(k >= 1)
        def _():
            give_back(k).start()

    SH = S // 2
    sh, sl = lax.div(s, 2), lax.rem(s, 2)

    def block(h):
        return mix_all.at[2 * h + sl]

    def rise(j):
        return remote(mix if j == 0 else block(sh - j), block(sh - j), us.at[j], ur.at[j + 1], (s + 2, t))

    def sink(j):
        return remote(mix if j == 0 else block(sh + j), block(sh + j), vs.at[j], vr.at[j + 1], (s - 2, t))

    def side(h, value=None):
        return remote(block(h) if value is None else value, block(h), ys.at[h], yr.at[h], (2 * sh + 1 - sl, t))

    def mix_step(j):
        if j == 0:
            side(sh, mix).start()

            @pl.when(sh < SH - 1)
            def _():
                rise(0).start()

            @pl.when(sh > 0)
            def _():
                sink(0).start()

            return

        @pl.when(sh >= j)
        def _():
            remote(block(sh - j), block(sh - j), us.at[j], ur.at[j], (s, mate)).wait_recv()

            @pl.when(sh < SH - 1)
            def _():
                rise(j).start()

            side(sh - j).start()

        @pl.when(sh + j < SH)
        def _():
            remote(block(sh + j), block(sh + j), vs.at[j], vr.at[j], (s, mate)).wait_recv()

            @pl.when(sh > 0)
            def _():
                sink(j).start()

            side(sh + j).start()

    def mix_finish():
        keep_mix.wait()
        for j in range(SH - 1):

            @pl.when((sh >= j) & (sh < SH - 1))
            def _():
                rise(j).wait_send()

            @pl.when((sh + j < SH) & (sh > 0))
            def _():
                sink(j).wait_send()

        def one(h):
            side(h).wait_send()
            side(h).wait_recv()

        each(0, SH, one)

    keep_mix = pltpu.make_async_copy(mix, mix_all.at[s], gsem.at[3])
    keep = pltpu.make_async_copy(rstage.at[0], back.at[s], rts.at[0])

    each(1, S, lambda i: send(0, at(i)))
    own(0)
    mix[...] = (out_gate[...].astype(jnp.float32) * conv_out[...].astype(jnp.float32)).astype(jnp.bfloat16)
    own(1)
    for copy in weights:
        copy.wait()
    project(0)

    def first(i):
        @pl.when(i < S)
        def _():
            forward(0, at(i))
            send(1, at(i))

        @pl.when((i >= 2) & (i < S + 1))
        def _():
            forward_on(0, at(i - 1))

        @pl.when(i >= 3)
        def _():
            complete(0, at(i - 2))
            project(at(i - 2))

    each(1, S + 2, first)
    mix_step(0)
    gradients(0, 0)

    def second(i):
        @pl.when(i < S)
        def _():
            forward(1, at(i))

        @pl.when((i >= 2) & (i < S + 1))
        def _():
            forward_on(1, at(i - 1))

        @pl.when((i >= 3) & (i < S + 3))
        def _():
            reduce_chip(i - 3, at(i - 3))

        @pl.when((i >= 3) & (i < S + 2))
        def _():
            complete(1, at(i - 2))
            gradients(i - 2, at(i - 2))

        @pl.when(i >= 4)
        def _():
            reduce_all(i - 4, at(i - 4))

        for j in range(1, SH):

            @pl.when(i == 2 * j)
            def _():
                mix_step(j)

    each(1, S + 4, second)
    keep.start()
    keep_mix.start()

    tile = min(512, Q)
    per = Q // tile

    def weight_grads(i):
        q, c = lax.div(i, per), pl.multiple_of(lax.rem(i, per) * tile, tile)
        x = rows[0, :, q, :, pl.ds(c, tile)].reshape(S * cap, tile)
        start = pl.multiple_of(q * Q + c, tile)
        gout[pl.ds(start, tile), :] = dot(x, ggu[...].reshape(S * cap, 2 * H), TN).astype(jnp.bfloat16)
        d = rows[1, :, q, :, pl.ds(c, tile)].reshape(S * cap, tile)
        gdown[:, pl.ds(start, tile)] = dot(hid[...].reshape(S * cap, H), d, TN).astype(jnp.bfloat16)

    each(0, T * per, weight_grads)
    results = [
        pltpu.make_async_copy(gout.at[:, pl.ds(0, H)], gwg_h, gsem.at[0]),
        pltpu.make_async_copy(gout.at[:, pl.ds(H, H)], gwu_h, gsem.at[1]),
        pltpu.make_async_copy(gdown, gwd_h, gsem.at[2]),
    ]
    for copy in results:
        copy.start()

    half(S - 2).wait_send()
    half(S - 1).wait_send()

    def finish(k):
        for a in range(2):
            direct(a, k).wait_send()
            to_mate(a, k).wait_send()
            for j in range(1, TH):
                across(a, j, k).wait_send()
                on_to_mate(a, j, k).wait_send()
        give_back(k).wait_send()
        give_back(k).wait_recv()

    each(1, S, finish)

    def finish_sums(k):
        for j in range(1, TH):
            chip_sum(j, k).wait_send()

    each(0, S, finish_sums)
    keep.wait()
    mix_finish()
    for copy in results:
        copy.wait()


def mixer_kernel(
    S, T, placed, cot, out_gate, conv_out, in_gate, conv_in, taps, back_h, mix_h, w_out_h,
    gwo, gci, gig, gog,
    back, mix, w_out, total, res, colst, cols, conv, after,
    lsem, ds, dr, m1s, m1r, xs, xr, m2s, m2r, bs, br,
):
    TH = T // 2
    cap, Q = back.shape[1], back.shape[2]
    tok = cot.shape[0]
    piece, group = Q // S, T * Q // S
    s, t, th, tl = spot()
    mate = 2 * th + 1 - tl
    local = [
        pltpu.make_async_copy(src, dst, lsem.at[n])
        for n, (src, dst) in enumerate(((back_h, back), (mix_h, mix), (w_out_h, w_out)))
    ]
    for copy in local:
        copy.start()
    greet(S, TH)

    def other(j):
        return lax.rem(th + j, TH)

    def behind(j):
        return lax.rem(th - j + TH, TH)

    def at(i):
        return partner(S, s, i)

    def direct(k):
        peer = flip(S, s, k)
        return remote(colst.at[peer], cols.at[s, t], ds.at[k], dr.at[k], (peer, t))

    def block(k, q):
        return cols.at[flip(S, s, k), q] if k is not None else res.at[q]

    def to_mate(k):
        n = S if k is None else k
        return remote(block(k, t), block(k, t), m1s.at[n], m1r.at[n], (s, mate))

    def across(j, k):
        n = S if k is None else k
        return remote(block(k, t), block(k, t), xs.at[j, n], xr.at[j, n], (s, 2 * other(j) + tl))

    def on_to_mate(j, k):
        n = S if k is None else k
        q = 2 * behind(j) + tl
        return remote(block(k, q), block(k, q), m2s.at[j, n], m2r.at[j, n], (s, mate))

    def forward(k):
        for j in range(1, TH):
            across(j, k).start()
        to_mate(k).start()

    def forward_on(k):
        for j in range(1, TH):
            across(j, k).wait_recv()
            on_to_mate(j, k).start()

    def complete(k):
        to_mate(k).wait_recv()
        for j in range(1, TH):
            on_to_mate(j, k).wait_recv()

    def sent(k):
        to_mate(k).wait_send()
        for j in range(1, TH):
            across(j, k).wait_send()
            on_to_mate(j, k).wait_send()

    local[0].wait()
    total[...] = dot(placed[...].reshape(S * cap, tok), back[...].reshape(S * cap, Q), TN)
    for q in range(T):

        @pl.when(t == q)
        def _():
            for g in range(S):
                columns = pl.ds(g * piece, piece)
                mine = cot[:, pl.ds(g * group + q * piece, piece)].astype(jnp.float32)
                value = (mine + total[:, columns]).astype(jnp.bfloat16)
                res[q, :, columns] = value
                colst[g] = value

    forward(None)
    each(1, S, lambda i: direct(at(i)).start())
    cols[s, t] = colst[s]
    forward(0)

    def arrive(i):
        direct(at(i)).wait_recv()
        forward(at(i))

    local[2].wait()
    forward_on(None)
    each(1, S, arrive)
    complete(None)
    grad_mixed = jnp.zeros((tok, w_out.shape[1]), jnp.float32)
    for g in range(S):
        some = jnp.concatenate([res[q, :, pl.ds(g * piece, piece)] for q in range(T)], axis=1)
        grad_mixed = grad_mixed + dot(some, w_out[pl.ds(g * group, group), :])
    gog[...] = (grad_mixed * conv_out[...].astype(jnp.float32)).astype(jnp.bfloat16)
    conv[pl.ds(0, tok), :] = grad_mixed * out_gate[...].astype(jnp.float32)

    def edge(target):
        return remote(conv.at[pl.ds(0, 8), :], after, bs.at[0], br.at[0], (target, t))

    @pl.when(s > 0)
    def _():
        edge(s - 1).start()

    local[1].wait()

    def take(k):
        complete(k)
        b = flip(S, s, k)
        columns = jnp.concatenate([cols[b, q] for q in range(T)], axis=1)
        gwo[...] += dot(columns, mix[b], TN)

    gwo[...] = jnp.zeros_like(gwo)
    forward_on(0)

    def step(i):
        @pl.when(i < S)
        def _():
            forward_on(at(i))

        take(at(i - 1))

    each(1, S + 1, step)

    @pl.when(s < S - 1)
    def _():
        edge(0).wait_recv()
        conv[pl.ds(tok, 8), :] = after[...]

    @pl.when(s == S - 1)
    def _():
        conv[pl.ds(tok, 8), :] = jnp.zeros_like(after)

    grad_g = (
        taps[2:3, :] * conv[pl.ds(0, tok), :]
        + taps[1:2, :] * conv[pl.ds(1, tok), :]
        + taps[0:1, :] * conv[pl.ds(2, tok), :]
    )
    gci[...] = (grad_g * in_gate[...].astype(jnp.float32)).astype(jnp.bfloat16)
    gig[...] = (grad_g * conv_in[...].astype(jnp.float32)).astype(jnp.bfloat16)

    @pl.when(s > 0)
    def _():
        edge(s - 1).wait_send()

    sent(None)
    each(0, S, sent)
    each(1, S, lambda k: direct(k).wait_send())


def expert_exchange(S, T, cap, inp, cot, placed, slot_w, out_gate, conv_out, w_gate, w_up, w_down):
    tok, D = inp.shape
    H = w_down.shape[0]
    TH, Q, SH = T // 2, D // T, S // 2
    bf, f32 = jnp.bfloat16, jnp.float32
    dma = pltpu.SemaphoreType.DMA
    vmem = pl.BlockSpec(memory_space=pltpu.VMEM)
    hbm = pl.BlockSpec(memory_space=pl.ANY)
    rows = S * cap
    return pl.pallas_call(
        functools.partial(expert_kernel, S, T),
        name="expert_exchange",
        out_shape=(
            jax.ShapeDtypeStruct((S, cap, Q), bf),
            jax.ShapeDtypeStruct((S,) + out_gate.shape, bf),
            jax.ShapeDtypeStruct((D, H), bf),
            jax.ShapeDtypeStruct((D, H), bf),
            jax.ShapeDtypeStruct((H, D), bf),
        ),
        in_specs=[vmem] * 6 + [hbm] * 3,
        out_specs=(hbm,) * 5,
        scratch_shapes=[
            pltpu.VMEM(out_gate.shape, bf),
            pltpu.VMEM((2, S, T, cap, Q), bf),
            pltpu.VMEM((2, S, cap, Q), bf),
            pltpu.VMEM((D, 2 * H), bf),
            pltpu.VMEM((H, D), bf),
            pltpu.VMEM((S, cap, 2 * H), f32),
            pltpu.VMEM((S, cap, H), bf),
            pltpu.VMEM((S, cap, 2 * H), bf),
            pltpu.VMEM((2, 2, TH, cap, Q), f32),
            pltpu.VMEM((S, TH, cap, Q), f32),
            pltpu.VMEM((2, cap, Q), f32),
            pltpu.VMEM((2, TH, NEAR, cap, Q), bf),
            pltpu.VMEM((TH, S, cap, Q), bf),
            pltpu.VMEM((TH, S, cap, Q), bf),
            pltpu.VMEM((S, cap, Q), bf),
            pltpu.VMEM((D, 2 * H), bf),
            pltpu.VMEM((H, D), bf),
            dma((3,)), dma((4,)),
            dma((2, S)), dma((2, S)),
            dma((2, S)), dma((2, S)),
            dma((2, TH, S)), dma((2, TH, S)),
            dma((2, TH, S)), dma((2, TH, S)),
            dma((S,)), dma((S,)),
            dma((TH, S)), dma((TH, S)),
            dma((S,)), dma((S,)),
            dma((SH,)), dma((SH + 1,)),
            dma((SH,)), dma((SH + 1,)),
            dma((SH,)), dma((SH,)),
        ],
        cost_estimate=pl.CostEstimate(
            flops=16 * rows * D * H, bytes_accessed=8 * rows * D + 24 * D * H, transcendentals=rows * H
        ),
        compiler_params=pltpu.CompilerParams(
            collective_id=0, has_side_effects=True, vmem_limit_bytes=67_043_328
        ),
    )(inp, cot, placed, slot_w, out_gate, conv_out, w_gate, w_up, w_down)


def mixer(S, T, placed, cot, out_gate, conv_out, in_gate, conv_in, taps, back, mix_all, w_out):
    tok, D = cot.shape
    B = w_out.shape[1]
    cap = placed.shape[1]
    TH, Q = T // 2, D // T
    bf, f32 = jnp.bfloat16, jnp.float32
    dma = pltpu.SemaphoreType.DMA
    vmem = pl.BlockSpec(memory_space=pltpu.VMEM)
    hbm = pl.BlockSpec(memory_space=pl.ANY)
    small = jax.ShapeDtypeStruct((tok, B), bf)
    return pl.pallas_call(
        functools.partial(mixer_kernel, S, T),
        name="mixer",
        out_shape=(jax.ShapeDtypeStruct((D // S, B), f32), small, small, small),
        in_specs=[vmem] * 7 + [hbm] * 3,
        out_specs=(vmem,) * 4,
        scratch_shapes=[
            pltpu.VMEM((S, cap, Q), bf),
            pltpu.VMEM((S, tok, B), bf),
            pltpu.VMEM((D, B), bf),
            pltpu.VMEM((tok, Q), f32),
            pltpu.VMEM((T, tok, Q), bf),
            pltpu.VMEM((S, tok, Q // S), bf),
            pltpu.VMEM((S, T, tok, Q // S), bf),
            pltpu.VMEM((tok + 8, B), f32),
            pltpu.VMEM((8, B), f32),
            dma((3,)),
            dma((S,)), dma((S,)),
            dma((S + 1,)), dma((S + 1,)),
            dma((TH, S + 1)), dma((TH, S + 1)),
            dma((TH, S + 1)), dma((TH, S + 1)),
            dma((1,)), dma((1,)),
        ],
        cost_estimate=pl.CostEstimate(
            flops=2 * tok * D * B * 2 + 2 * S * cap * tok * Q, bytes_accessed=4 * D * B, transcendentals=0
        ),
        compiler_params=pltpu.CompilerParams(
            collective_id=1, has_side_effects=True, vmem_limit_bytes=67_043_328
        ),
    )(placed, cot, out_gate, conv_out, in_gate, conv_in, taps, back, mix_all, w_out)


def slot_masks(routes, route_weight, experts, capacity):
    tok_rows = routes.shape[0]
    names = jnp.arange(experts, dtype=jnp.int32)
    hits = routes[None, :, :] == names[:, None, None]
    chosen = jnp.any(hits, axis=2)
    weight = jnp.sum(jnp.where(hits, route_weight[None], 0.0), axis=2)
    order = jnp.arange(tok_rows, dtype=jnp.int32)
    before = (order[:, None] < order[None, :]).astype(jnp.bfloat16)
    rank = jnp.dot(chosen.astype(jnp.bfloat16), before, preferred_element_type=jnp.float32)
    rank = jnp.where(chosen, rank.astype(jnp.int32), -1)
    slots = jnp.arange(capacity, dtype=jnp.int32)
    placed = rank[:, None, :] == slots[None, :, None]
    slot_weight = jnp.sum(jnp.where(placed, weight[:, None, :], 0.0), axis=2, keepdims=True)
    return placed.astype(jnp.bfloat16), slot_weight


def per_device(
    cotangent, moe_input, routes, route_weight, conv_input, input_gate, output_gate, conv_output,
    taps, w_out, w_gate, w_up, w_down,
):
    experts = lax.axis_size("sp")
    tp_size = lax.axis_size("tp")
    tok_rows, top_k = routes.shape
    capacity = -(-max(2, 2 * tok_rows * top_k // experts) // 16) * 16
    placed, slot_weight = slot_masks(routes, route_weight, experts, capacity)
    returned, mixed_all, gate_wgrad, up_wgrad, grad_down = expert_exchange(
        experts, tp_size, capacity, moe_input, cotangent, placed, slot_weight, output_gate, conv_output,
        w_gate[0], w_up[0], w_down[0],
    )
    grad_w_out, grad_conv_input, grad_input_gate, grad_output_gate = mixer(
        experts, tp_size, placed, cotangent, output_gate, conv_output, input_gate, conv_input, taps,
        returned, mixed_all, w_out,
    )
    return (
        gate_wgrad[None], up_wgrad[None], grad_down[None], grad_w_out,
        grad_conv_input, grad_input_gate, grad_output_gate,
    )


def solution(mesh):
    return jax.shard_map(
        per_device,
        mesh=mesh,
        in_specs=(
            P("sp", None), P("sp", None), P("sp", None), P("sp", None),
            P("sp", "tp"), P("sp", "tp"), P("sp", "tp"), P("sp", "tp"),
            P(None, "tp"), P(None, "tp"),
            P("sp", None, "tp"), P("sp", None, "tp"), P("sp", "tp", None),
        ),
        out_specs=(
            P("sp", None, "tp"), P("sp", None, "tp"), P("sp", "tp", None),
            P("sp", "tp"), P("sp", "tp"), P("sp", "tp"), P("sp", "tp"),
        ),
        check_vma=False,
    )
```

time: 261 us -> 202 us (0.77)
  waiting for transfers between devices: 42.6 us -> 0 us
  Pallas kernels: 157 us -> 187 us
  between operations: 14.1 us -> 0.67 us
  starting transfers between devices: 12.1 us -> 0 us
  matrix products: 10.9 us -> 0.14 us
  local copies, waits for them, and re-layouts: 18.6 us -> 11.6 us
    pallas_call x0 -> x1, Pallas kernels: none -> 26.5 us  [mixer(): pl.pallas_call(functools.partial(mixer_kernel, S, T), name='mixer', out_s...]
    all_gather x2 -> x0, waiting for transfers between devices: 21.5 us -> none  [the longest x1 13.5 us: per_device(): resid_cols = lax.all_gather(own, 'tp', axis=2, tiled=True)]
    all_to_all x2 -> x0, waiting for transfers between devices: 14.2 us -> none  [over_sp(): return lax.all_to_all(value, 'sp', split_axis=0, concat_axis=0, tiled=True)]
    dot_general x3 -> x0, matrix products: 10.8 us -> none  [the longest x1 4.33 us: per_device(): jnp.dot(resid_grad, out_turned, preferred_element_type=jnp.float32)]
    all_to_all x2 -> x0, starting transfers between devices: 10.8 us -> none  [over_sp(): return lax.all_to_all(value, 'sp', split_axis=0, concat_axis=0, tiled=True)]
    transpose x2 -> x0, local copies, waits for them, and re-layouts: 6.73 us -> none  [the longest x1 4.91 us: per_device(): w_out.reshape(experts, tp_size, piece, -1).swapaxes(0, 1)]
    ppermute x1 -> x0, waiting for transfers between devices: 6.13 us -> none  [from_behind(): lax.ppermute(value, axis, [(source, source + steps) for source in range(l...]
    unnamed x23 -> x19, local copies, waits for them, and re-layouts: 6.04 us -> 10.6 us
  transfers between devices with their start and end apart: 5 -> 0, of which waited for: 4 -> 0; matrix products, arithmetic and copies ran while one was open for 5% -> 0% of each run, Pallas kernels for 0% -> 0%
where the time goes in v2:
time: 202 us
  Pallas kernels  187 us (93%)
  local copies, waits for them, and re-layouts  11.6 us (6%)
  other arithmetic  2.46 us (1%)
    pallas_call x1, Pallas kernels, expert_exchange(): pl.pallas_call(functools.partial(expert_kernel, S, T), name='expert_excha...  161 us
    pallas_call x1, Pallas kernels, mixer(): pl.pallas_call(functools.partial(mixer_kernel, S, T), name='mixer', out_s...  26.5 us
    unnamed x19, local copies, waits for them, and re-layouts  10.6 us

profile of v2, /device:TPU:0, one launch (start us, length us, event | category | flops | bytes accessed | tf_op | source)
XLA Modules:
  0.0 202.0 jit_solution(5127308700186957300)
XLA Ops:
  0.6 0.7 fusion.2
  1.3 0.1 fusion
  1.5 0.8 fusion.1.placed
  2.3 0.7 select_reduce_fusion.1
  3.0 0.2 select_reduce_fusion
  3.2 0.9 copy.25.slot_w
  4.2 160.6 %expert_exchange.1 = (bf16[8,96,1024]{2,1,0:T(8,128)(2,1)}, bf16[8,192,512]{2,1,0:T(8,128)(2,1)}, bf16[4096,256]{1,0:T(8,128)(2,1)}, bf16[4096,256]{1,0:T(8,128)(2,1)}, bf16[256,4096]{1,0:T(8,128)(2,1)}) custom-call(bf16[192,4096]{1,0:T(8,128)(2,1)} %inp.1, bf16[192,4096]{1,0:T(8,128)(2,1)} %cot.3, bf16[8,96,192]{2,1,0:T(8,128)(2,1)} %fusion.1.placed, ...), custom_call_target="tpu_custom_call" | custom-call | flops 12884901888 | bytes 50331648 | tf_op jit(solution)/shard_map/expert_exchange/pallas_call | solution.py:568
  164.8 26.5 %mixer.1 = (f32[512,512]{1,0:T(8,128)}, bf16[192,512]{1,0:T(8,128)(2,1)}, bf16[192,512]{1,0:T(8,128)(2,1)}, bf16[192,512]{1,0:T(8,128)(2,1)}) custom-call(bf16[8,96,192]{2,1,0:T(8,128)(2,1)} %fusion.1.placed, bf16[192,4096]{1,0:T(8,128)(2,1)} %cot.3, bf16[192,512]{1,0:T(8,128)(2,1)} %out_gate.3, bf16[192,512]{1,0:T(8,128)(2,1)} %conv_out.3, ...), custom_call_target="tpu_custom_call" | custom-call | flops 1912602624 | bytes 8388608 | tf_op jit(solution)/shard_map/mixer/pallas_call | solution.py:629
  191.3 0.0 copy-start.1
  191.3 3.2 %copy.33 = bf16[1,4096,256]{2,1,0:T(8,128)(2,1)} copy(bf16[1,4096,256]{2,1,0:T(8,128)(2,1)} %bitcast.10) | data formatting | bytes 4194304
  194.5 0.0 copy-done.1
  194.5 0.0 copy-start
  194.5 1.3 copy.34
  195.9 1.0 copy-done
  196.9 0.0 copy-start.2
  196.9 1.3 copy.35
  198.2 0.6 copy-done.2
  198.8 0.0 copy-start.5
  198.8 0.0 copy-start.4
  198.8 0.0 copy-start.3
  198.9 1.0 copy.36
  199.8 0.1 copy-done.5
  199.9 0.7 copy.37
  200.6 0.0 copy-done.4
  200.6 0.7 copy.38
  201.3 0.0 copy-done.3
  201.3 0.7 copy.39
Async XLA Ops:
  191.3 3.2 %copy-start.1 = (bf16[4096,256]{1,0:T(8,128)(2,1)S(1)}, bf16[4096,256]{1,0:T(8,128)(2,1)}, u32[]{:S(2)}) copy-start(bf16[4096,256]{1,0:T(8,128)(2,1)} %get-tuple-element.17) | copy-start | bytes 6291460
  194.5 2.3 %copy-start = (bf16[256,4096]{1,0:T(8,128)(2,1)S(1)}, bf16[256,4096]{1,0:T(8,128)(2,1)}, u32[]{:S(2)}) copy-start(bf16[256,4096]{1,0:T(8,128)(2,1)} %get-tuple-element.18) | copy-start | bytes 6291460
  196.9 2.0 copy-start.2
  198.8 1.1 copy-start.5
  198.8 1.8 copy-start.4
  198.8 2.4 %copy-start.3 = (bf16[192,512]{1,0:T(8,128)(2,1)S(1)}, bf16[192,512]{1,0:T(8,128)(2,1)}, u32[]{:S(2)}) copy-start(bf16[192,512]{1,0:T(8,128)(2,1)} %get-tuple-element.38) | copy-start | bytes 589828

commit v3 on v2

--- a/solution.py
+++ b/solution.py
@@ -7,7 +7,8 @@
 from jax.experimental.pallas import tpu as pltpu
 from jax.sharding import PartitionSpec as P
 
-NEAR = 2
+NEAR = 4
+LAG = 1
 MESH = pl.DeviceIdType.MESH
 NN = (((1,), (0,)), ((), ()))
 NT = (((1,), (1,)), ((), ()))
@@ -96,6 +97,10 @@
     def at(i):
         return partner(S, s, i)
 
+    def then(i):
+        far = S - S // 2
+        return jnp.where(i <= far, at(i + S // 2 - 1), at(i - far))
+
     weights = [
         pltpu.make_async_copy(wg_h, wgu.at[:, pl.ds(0, H)], wsem.at[0]),
         pltpu.make_async_copy(wu_h, wgu.at[:, pl.ds(H, H)], wsem.at[1]),
@@ -212,10 +217,10 @@
             o = other(j)
             xsend[j, k] = (part[slot, tl, o] + matebuf[n, o]).astype(jnp.bfloat16)
             chip_sum(j, k).start()
-        total_part[slot] = part[slot, tl, th] + matebuf[n, th]
+        total_part[lax.rem(n, 3)] = part[slot, tl, th] + matebuf[n, th]
 
     def reduce_all(n, k):
-        total = total_part[lax.rem(n, 2)]
+        total = total_part[lax.rem(n, 3)]
         for j in range(1, TH):
             chip_sum(j, k).wait_recv()
             total = total + xrecv[j, k].astype(jnp.float32)
@@ -302,12 +307,24 @@
     for copy in weights:
         copy.wait()
     project(0)
+    gradients(0, 0)
 
     def first(i):
+        @pl.when(i == 3)
+        def _():
+            reduce_chip(0, 0)
+
+        @pl.when(i == 4)
+        def _():
+            reduce_all(0, 0)
+
         @pl.when(i < S)
         def _():
             forward(0, at(i))
-            send(1, at(i))
+
+        @pl.when((i >= LAG) & (i < S))
+        def _():
+            send(1, then(i - LAG + 1))
 
         @pl.when((i >= 2) & (i < S + 1))
         def _():
@@ -319,30 +336,30 @@
             project(at(i - 2))
 
     each(1, S + 2, first)
+    each(max(1, S - LAG + 1), S, lambda i: send(1, then(i)))
     mix_step(0)
-    gradients(0, 0)
 
     def second(i):
         @pl.when(i < S)
         def _():
-            forward(1, at(i))
+            forward(1, then(i))
 
         @pl.when((i >= 2) & (i < S + 1))
         def _():
-            forward_on(1, at(i - 1))
-
-        @pl.when((i >= 3) & (i < S + 3))
-        def _():
-            reduce_chip(i - 3, at(i - 3))
+            forward_on(1, then(i - 1))
 
         @pl.when((i >= 3) & (i < S + 2))
         def _():
-            complete(1, at(i - 2))
-            gradients(i - 2, at(i - 2))
-
-        @pl.when(i >= 4)
-        def _():
-            reduce_all(i - 4, at(i - 4))
+            complete(1, then(i - 2))
+            gradients(i - 2, then(i - 2))
+
+        @pl.when((i >= 4) & (i < S + 3))
+        def _():
+            reduce_chip(i - 3, then(i - 3))
+
+        @pl.when(i >= 6)
+        def _():
+            reduce_all(i - 5, then(i - 5))
 
         for j in range(1, SH):
 
@@ -350,7 +367,7 @@
             def _():
                 mix_step(j)
 
-    each(1, S + 4, second)
+    each(1, S + 5, second)
     keep.start()
     keep_mix.start()
 
@@ -588,7 +605,7 @@
             pltpu.VMEM((S, cap, 2 * H), bf),
             pltpu.VMEM((2, 2, TH, cap, Q), f32),
             pltpu.VMEM((S, TH, cap, Q), f32),
-            pltpu.VMEM((2, cap, Q), f32),
+            pltpu.VMEM((3, cap, Q), f32),
             pltpu.VMEM((2, TH, NEAR, cap, Q), bf),
             pltpu.VMEM((TH, S, cap, Q), bf),
             pltpu.VMEM((TH, S, cap, Q), bf),

time: 202 us -> 185 us (0.916)
  Pallas kernels: 187 us -> 170 us
    pallas_call x1, Pallas kernels: 161 us -> 143 us  [expert_exchange(): pl.pallas_call(functools.partial(expert_kernel, S, T), name='expert_excha...]
where the time goes in v3:
time: 185 us
  Pallas kernels  170 us (92%)
  local copies, waits for them, and re-layouts  11.6 us (6%)
  other arithmetic  2.46 us (1%)
    pallas_call x1, Pallas kernels, expert_exchange(): pl.pallas_call(functools.partial(expert_kernel, S, T), name='expert_excha...  143 us
    pallas_call x1, Pallas kernels, mixer(): pl.pallas_call(functools.partial(mixer_kernel, S, T), name='mixer', out_s...  26.9 us
    unnamed x19, local copies, waits for them, and re-layouts  10.6 us

profile of v3, /device:TPU:0, one launch (start us, length us, event | category | flops | bytes accessed | tf_op | source)
XLA Modules:
  0.0 184.8 jit_solution(5178113311132355090)
XLA Ops:
  0.6 0.7 fusion.2
  1.3 0.1 fusion
  1.5 0.8 fusion.1.placed
  2.3 0.7 select_reduce_fusion.1
  3.0 0.2 select_reduce_fusion
  3.2 0.9 copy.25.slot_w
  4.2 143.1 %expert_exchange.1 = (bf16[8,96,1024]{2,1,0:T(8,128)(2,1)}, bf16[8,192,512]{2,1,0:T(8,128)(2,1)}, bf16[4096,256]{1,0:T(8,128)(2,1)}, bf16[4096,256]{1,0:T(8,128)(2,1)}, bf16[256,4096]{1,0:T(8,128)(2,1)}) custom-call(bf16[192,4096]{1,0:T(8,128)(2,1)} %inp.1, bf16[192,4096]{1,0:T(8,128)(2,1)} %cot.3, bf16[8,96,192]{2,1,0:T(8,128)(2,1)} %fusion.1.placed, ...), custom_call_target="tpu_custom_call" | custom-call | flops 12884901888 | bytes 50331648 | tf_op jit(solution)/shard_map/expert_exchange/pallas_call | solution.py:585
  147.3 26.9 %mixer.1 = (f32[512,512]{1,0:T(8,128)}, bf16[192,512]{1,0:T(8,128)(2,1)}, bf16[192,512]{1,0:T(8,128)(2,1)}, bf16[192,512]{1,0:T(8,128)(2,1)}) custom-call(bf16[8,96,192]{2,1,0:T(8,128)(2,1)} %fusion.1.placed, bf16[192,4096]{1,0:T(8,128)(2,1)} %cot.3, bf16[192,512]{1,0:T(8,128)(2,1)} %out_gate.3, bf16[192,512]{1,0:T(8,128)(2,1)} %conv_out.3, ...), custom_call_target="tpu_custom_call" | custom-call | flops 1912602624 | bytes 8388608 | tf_op jit(solution)/shard_map/mixer/pallas_call | solution.py:646
  174.1 0.0 copy-start.1
  174.1 3.2 %copy.33 = bf16[1,4096,256]{2,1,0:T(8,128)(2,1)} copy(bf16[1,4096,256]{2,1,0:T(8,128)(2,1)} %bitcast.10) | data formatting | bytes 4194304
  177.3 0.0 copy-done.1
  177.3 0.0 copy-start
  177.3 1.3 copy.34
  178.7 1.0 copy-done
  179.7 0.0 copy-start.2
  179.7 1.3 copy.35
  181.0 0.6 copy-done.2
  181.7 0.0 copy-start.5
  181.7 0.0 copy-start.4
  181.7 0.0 copy-start.3
  181.7 1.0 copy.36
  182.6 0.1 copy-done.5
  182.7 0.7 copy.37
  183.4 0.0 copy-done.4
  183.4 0.7 copy.38
  184.1 0.0 copy-done.3
  184.1 0.7 copy.39
Async XLA Ops:
  174.1 3.2 %copy-start.1 = (bf16[4096,256]{1,0:T(8,128)(2,1)S(1)}, bf16[4096,256]{1,0:T(8,128)(2,1)}, u32[]{:S(2)}) copy-start(bf16[4096,256]{1,0:T(8,128)(2,1)} %get-tuple-element.17) | copy-start | bytes 6291460
  177.3 2.3 %copy-start = (bf16[256,4096]{1,0:T(8,128)(2,1)S(1)}, bf16[256,4096]{1,0:T(8,128)(2,1)}, u32[]{:S(2)}) copy-start(bf16[256,4096]{1,0:T(8,128)(2,1)} %get-tuple-element.18) | copy-start | bytes 6291460
  179.7 2.0 %copy-start.2 = (f32[512,512]{1,0:T(8,128)S(1)}, f32[512,512]{1,0:T(8,128)}, u32[]{:S(2)}) copy-start(f32[512,512]{1,0:T(8,128)} %get-tuple-element.35) | copy-start | bytes 3145732
  181.7 1.1 copy-start.5
  181.7 1.8 copy-start.4
  181.7 2.4 %copy-start.3 = (bf16[192,512]{1,0:T(8,128)(2,1)S(1)}, bf16[192,512]{1,0:T(8,128)(2,1)}, u32[]{:S(2)}) copy-start(bf16[192,512]{1,0:T(8,128)(2,1)} %get-tuple-element.38) | copy-start | bytes 589828

commit v4 on v3

--- a/solution.py
+++ b/solution.py
@@ -8,7 +8,6 @@
 from jax.sharding import PartitionSpec as P
 
 NEAR = 4
-LAG = 1
 MESH = pl.DeviceIdType.MESH
 NN = (((1,), (0,)), ((), ()))
 NT = (((1,), (1,)), ((), ()))
@@ -97,10 +96,6 @@
     def at(i):
         return partner(S, s, i)
 
-    def then(i):
-        far = S - S // 2
-        return jnp.where(i <= far, at(i + S // 2 - 1), at(i - far))
-
     weights = [
         pltpu.make_async_copy(wg_h, wgu.at[:, pl.ds(0, H)], wsem.at[0]),
         pltpu.make_async_copy(wu_h, wgu.at[:, pl.ds(H, H)], wsem.at[1]),
@@ -300,9 +295,13 @@
     keep_mix = pltpu.make_async_copy(mix, mix_all.at[s], gsem.at[3])
     keep = pltpu.make_async_copy(rstage.at[0], back.at[s], rts.at[0])
 
-    each(1, S, lambda i: send(0, at(i)))
+    mix[...] = (out_gate[...].astype(jnp.float32) * conv_out[...].astype(jnp.float32)).astype(jnp.bfloat16)
+    middle = max(2, S // 2)
+    each(middle, S, lambda i: send(0, at(i)))
+    mix_step(0)
+    each(1, middle, lambda i: send(0, at(i)))
+    each(1, middle, lambda i: send(1, at(i)))
     own(0)
-    mix[...] = (out_gate[...].astype(jnp.float32) * conv_out[...].astype(jnp.float32)).astype(jnp.bfloat16)
     own(1)
     for copy in weights:
         copy.wait()
@@ -310,43 +309,63 @@
     gradients(0, 0)
 
     def first(i):
-        @pl.when(i == 3)
+        @pl.when(i < S)
+        def _():
+            forward(0, at(i))
+
+        @pl.when(i == S - 1)
+        def _():
+            each(middle, S, lambda m: send(1, at(m)))
+
+        @pl.when(i == middle + 1)
         def _():
             reduce_chip(0, 0)
 
-        @pl.when(i == 4)
+        @pl.when(i == middle + 3)
         def _():
             reduce_all(0, 0)
 
-        @pl.when(i < S)
-        def _():
-            forward(0, at(i))
-
-        @pl.when((i >= LAG) & (i < S))
-        def _():
-            send(1, then(i - LAG + 1))
-
-        @pl.when((i >= 2) & (i < S + 1))
+        @pl.when((i >= middle + 1) & (i < S + 1))
         def _():
             forward_on(0, at(i - 1))
 
-        @pl.when(i >= 3)
+        @pl.when(i >= middle + 2)
         def _():
             complete(0, at(i - 2))
             project(at(i - 2))
 
-    each(1, S + 2, first)
-    each(max(1, S - LAG + 1), S, lambda i: send(1, then(i)))
-    mix_step(0)
+    each(middle, S + 2, first)
+    mix_step(1)
+
+    lead = S // 4
+
+    def near_at(i):
+        return (i > lead) & (i < lead + middle)
+
+    def then(i):
+        return jnp.where(i <= lead, at(i + middle - 1), jnp.where(i < lead + middle, at(i - lead), at(i)))
 
     def second(i):
+        @pl.when(near_at(i))
+        def _():
+            forward(0, then(i))
+
         @pl.when(i < S)
         def _():
             forward(1, then(i))
 
+        @pl.when(near_at(i - 1))
+        def _():
+            forward_on(0, then(i - 1))
+
         @pl.when((i >= 2) & (i < S + 1))
         def _():
             forward_on(1, then(i - 1))
+
+        @pl.when(near_at(i - 2))
+        def _():
+            complete(0, then(i - 2))
+            project(then(i - 2))
 
         @pl.when((i >= 3) & (i < S + 2))
         def _():
@@ -361,9 +380,9 @@
         def _():
             reduce_all(i - 5, then(i - 5))
 
-        for j in range(1, SH):
-
-            @pl.when(i == 2 * j)
+        for j in range(2, SH):
+
+            @pl.when(i == S // 2 + 1 + (S // 2) * (j - 1) // (SH - 1))
             def _():
                 mix_step(j)
 
@@ -420,7 +439,7 @@
 def mixer_kernel(
     S, T, placed, cot, out_gate, conv_out, in_gate, conv_in, taps, back_h, mix_h, w_out_h,
     gwo, gci, gig, gog,
-    back, mix, w_out, total, res, colst, cols, conv, after,
+    back, mix, w_out, total, res, colst, near, cols, conv, after,
     lsem, ds, dr, m1s, m1r, xs, xr, m2s, m2r, bs, br,
 ):
     TH = T // 2
@@ -450,6 +469,11 @@
         peer = flip(S, s, k)
         return remote(colst.at[peer], cols.at[s, t], ds.at[k], dr.at[k], (peer, t))
 
+    def direct_too(j, k):
+        peer = flip(S, s, k)
+        land = cols.at[s, 2 * other(j) + tl]
+        return remote(near.at[j, k], land, xs.at[j, k], xr.at[TH - j, k], (peer, t))
+
     def block(k, q):
         return cols.at[flip(S, s, k), q] if k is not None else res.at[q]
 
@@ -467,8 +491,11 @@
         return remote(block(k, q), block(k, q), m2s.at[j, n], m2r.at[j, n], (s, mate))
 
     def forward(k):
-        for j in range(1, TH):
-            across(j, k).start()
+        @pl.when((S if k is None else k) >= NEAR)
+        def _():
+            for j in range(1, TH):
+                across(j, k).start()
+
         to_mate(k).start()
 
     def forward_on(k):
@@ -502,8 +529,6 @@
 
     forward(None)
     each(1, S, lambda i: direct(at(i)).start())
-    cols[s, t] = colst[s]
-    forward(0)
 
     def arrive(i):
         direct(at(i)).wait_recv()
@@ -513,6 +538,21 @@
     forward_on(None)
     each(1, S, arrive)
     complete(None)
+    for g in range(S):
+
+        @pl.when(s == g)
+        def _():
+            for q in range(T):
+                cols[s, q] = res[q, :, pl.ds(g * piece, piece)]
+
+        for k in range(1, min(NEAR, S)):
+
+            @pl.when(flip(S, s, k) == g)
+            def _():
+                for j in range(1, TH):
+                    near[j, k] = res[2 * other(j) + tl, :, pl.ds(g * piece, piece)]
+                    direct_too(j, k).start()
+
     grad_mixed = jnp.zeros((tok, w_out.shape[1]), jnp.float32)
     for g in range(S):
         some = jnp.concatenate([res[q, :, pl.ds(g * piece, piece)] for q in range(T)], axis=1)
@@ -530,20 +570,27 @@
     local[1].wait()
 
     def take(k):
-        complete(k)
+        @pl.when(k > 0)
+        def _():
+            complete(k)
         b = flip(S, s, k)
         columns = jnp.concatenate([cols[b, q] for q in range(T)], axis=1)
         gwo[...] += dot(columns, mix[b], TN)
 
     gwo[...] = jnp.zeros_like(gwo)
-    forward_on(0)
+    take(0)
+
+    def turn(i):
+        return at(jnp.where(i <= S - NEAR, i + NEAR - 1, i - (S - NEAR)))
 
     def step(i):
         @pl.when(i < S)
         def _():
-            forward_on(at(i))
-
-        take(at(i - 1))
+            forward_on(turn(i))
+
+        @pl.when(i >= 2)
+        def _():
+            take(turn(i - 1))
 
     each(1, S + 1, step)
 
@@ -569,7 +616,7 @@
         edge(s - 1).wait_send()
 
     sent(None)
-    each(0, S, sent)
+    each(1, S, sent)
     each(1, S, lambda k: direct(k).wait_send())
 
 
@@ -656,6 +703,7 @@
             pltpu.VMEM((tok, Q), f32),
             pltpu.VMEM((T, tok, Q), bf),
             pltpu.VMEM((S, tok, Q // S), bf),
+            pltpu.VMEM((TH, NEAR, tok, Q // S), bf),
             pltpu.VMEM((S, T, tok, Q // S), bf),
             pltpu.VMEM((tok + 8, B), f32),
             pltpu.VMEM((8, B), f32),

time: 185 us -> 174 us (0.941)
  Pallas kernels: 170 us -> 158 us
    pallas_call x1, Pallas kernels: 143 us -> 134 us  [expert_exchange(): pl.pallas_call(functools.partial(expert_kernel, S, T), name='expert_excha...]
    pallas_call x1, Pallas kernels: 26.9 us -> 24.8 us  [mixer(): pl.pallas_call(functools.partial(mixer_kernel, S, T), name='mixer', out_s...]
where the time goes in v4:
time: 174 us; the launch traced here: 173 us
  Pallas kernels  158 us (91%)
  local copies, waits for them, and re-layouts  11.6 us (7%)
  other arithmetic  2.46 us (1%)
    pallas_call x1, Pallas kernels, expert_exchange(): pl.pallas_call(functools.partial(expert_kernel, S, T), name='expert_excha...  134 us
    pallas_call x1, Pallas kernels, mixer(): pl.pallas_call(functools.partial(mixer_kernel, S, T), name='mixer', out_s...  24.8 us
    unnamed x19, local copies, waits for them, and re-layouts  10.6 us

profile of v4, /device:TPU:0, one launch (start us, length us, event | category | flops | bytes accessed | tf_op | source)
XLA Modules:
  0.0 173.3 jit_solution(17033512262388365872)
XLA Ops:
  0.6 0.7 fusion.2
  1.3 0.1 fusion
  1.5 0.8 fusion.1.placed
  2.3 0.7 select_reduce_fusion.1
  3.0 0.2 select_reduce_fusion
  3.2 0.9 copy.25.slot_w
  4.2 133.7 %expert_exchange.1 = (bf16[8,96,1024]{2,1,0:T(8,128)(2,1)}, bf16[8,192,512]{2,1,0:T(8,128)(2,1)}, bf16[4096,256]{1,0:T(8,128)(2,1)}, bf16[4096,256]{1,0:T(8,128)(2,1)}, bf16[256,4096]{1,0:T(8,128)(2,1)}) custom-call(bf16[192,4096]{1,0:T(8,128)(2,1)} %inp.1, bf16[192,4096]{1,0:T(8,128)(2,1)} %cot.3, bf16[8,96,192]{2,1,0:T(8,128)(2,1)} %fusion.1.placed, ...), custom_call_target="tpu_custom_call" | custom-call | flops 12884901888 | bytes 50331648 | tf_op jit(solution)/shard_map/expert_exchange/pallas_call | solution.py:632
  137.9 24.8 %mixer.1 = (f32[512,512]{1,0:T(8,128)}, bf16[192,512]{1,0:T(8,128)(2,1)}, bf16[192,512]{1,0:T(8,128)(2,1)}, bf16[192,512]{1,0:T(8,128)(2,1)}) custom-call(bf16[8,96,192]{2,1,0:T(8,128)(2,1)} %fusion.1.placed, bf16[192,4096]{1,0:T(8,128)(2,1)} %cot.3, bf16[192,512]{1,0:T(8,128)(2,1)} %out_gate.3, bf16[192,512]{1,0:T(8,128)(2,1)} %conv_out.3, ...), custom_call_target="tpu_custom_call" | custom-call | flops 1912602624 | bytes 8388608 | tf_op jit(solution)/shard_map/mixer/pallas_call | solution.py:693
  162.7 0.0 copy-start.1
  162.7 3.2 %copy.33 = bf16[1,4096,256]{2,1,0:T(8,128)(2,1)} copy(bf16[1,4096,256]{2,1,0:T(8,128)(2,1)} %bitcast.10) | data formatting | bytes 4194304
  165.9 0.0 copy-done.1
  165.9 0.0 copy-start
  165.9 1.3 copy.34
  167.2 1.0 copy-done
  168.3 0.0 copy-start.2
  168.3 1.3 copy.35
  169.6 0.6 copy-done.2
  170.2 0.0 copy-start.5
  170.2 0.0 copy-start.4
  170.2 0.0 copy-start.3
  170.2 1.0 copy.36
  171.2 0.1 copy-done.5
  171.3 0.7 copy.37
  172.0 0.0 copy-done.4
  172.0 0.7 copy.38
  172.7 0.0 copy-done.3
  172.7 0.7 copy.39
Async XLA Ops:
  162.7 3.2 %copy-start.1 = (bf16[4096,256]{1,0:T(8,128)(2,1)S(1)}, bf16[4096,256]{1,0:T(8,128)(2,1)}, u32[]{:S(2)}) copy-start(bf16[4096,256]{1,0:T(8,128)(2,1)} %get-tuple-element.17) | copy-start | bytes 6291460
  165.9 2.3 %copy-start = (bf16[256,4096]{1,0:T(8,128)(2,1)S(1)}, bf16[256,4096]{1,0:T(8,128)(2,1)}, u32[]{:S(2)}) copy-start(bf16[256,4096]{1,0:T(8,128)(2,1)} %get-tuple-element.18) | copy-start | bytes 6291460
  168.3 2.0 %copy-start.2 = (f32[512,512]{1,0:T(8,128)S(1)}, f32[512,512]{1,0:T(8,128)}, u32[]{:S(2)}) copy-start(f32[512,512]{1,0:T(8,128)} %get-tuple-element.35) | copy-start | bytes 3145732
  170.2 1.1 copy-start.5
  170.2 1.8 %copy-start.4 = (bf16[192,512]{1,0:T(8,128)(2,1)S(1)}, bf16[192,512]{1,0:T(8,128)(2,1)}, u32[]{:S(2)}) copy-start(bf16[192,512]{1,0:T(8,128)(2,1)} %get-tuple-element.37) | copy-start | bytes 589828
  170.2 2.4 %copy-start.3 = (bf16[192,512]{1,0:T(8,128)(2,1)S(1)}, bf16[192,512]{1,0:T(8,128)(2,1)}, u32[]{:S(2)}) copy-start(bf16[192,512]{1,0:T(8,128)(2,1)} %get-tuple-element.38) | copy-start | bytes 589828

commit v5 on v4

--- a/solution.py
+++ b/solution.py
@@ -8,6 +8,7 @@
 from jax.sharding import PartitionSpec as P
 
 NEAR = 4
+CUTS = 4
 MESH = pl.DeviceIdType.MESH
 NN = (((1,), (0,)), ((), ()))
 NT = (((1,), (1,)), ((), ()))
@@ -69,7 +70,7 @@
 
 
 def expert_kernel(
-    S, T, inp, cot, placed, slot_w, out_gate, conv_out, wg_h, wu_h, wd_h,
+    S, T, inp, cot, placed, weight, out_gate, conv_out, wg_h, wu_h, wd_h,
     back, mix_all, gwg_h, gwu_h, gwd_h,
     mix, rows, stage, wgu, wd, proj, hid, ggu, part, matebuf, total_part, near, xsend, xrecv, rstage, gout, gdown,
     wsem, gsem, ds, dr, m1s, m1r, xs, xr, m2s, m2r, r1s, r1r, r2s, r2r, rts, rtr, us, ur, vs, vr, ys, yr,
@@ -127,7 +128,7 @@
     def pick(a, e, columns):
         picked = dot(placed[e], source[a][:, columns])
         if a == 1:
-            picked = picked * slot_w[e]
+            picked = picked * jnp.sum(placed[e].astype(jnp.float32) * weight[pl.ds(e, 1), :], axis=1, keepdims=True)
         return picked.astype(jnp.bfloat16)
 
     def send(a, k):
@@ -437,8 +438,8 @@
 
 
 def mixer_kernel(
-    S, T, placed, cot, out_gate, conv_out, in_gate, conv_in, taps, back_h, mix_h, w_out_h,
-    gwo, gci, gig, gog,
+    S, T, placed, cot, out_gate, back_h, mix_h, w_out_h,
+    gwo, gm, shifted,
     back, mix, w_out, total, res, colst, near, cols, conv, after,
     lsem, ds, dr, m1s, m1r, xs, xr, m2s, m2r, bs, br,
 ):
@@ -557,7 +558,7 @@
     for g in range(S):
         some = jnp.concatenate([res[q, :, pl.ds(g * piece, piece)] for q in range(T)], axis=1)
         grad_mixed = grad_mixed + dot(some, w_out[pl.ds(g * group, group), :])
-    gog[...] = (grad_mixed * conv_out[...].astype(jnp.float32)).astype(jnp.bfloat16)
+    gm[...] = grad_mixed
     conv[pl.ds(0, tok), :] = grad_mixed * out_gate[...].astype(jnp.float32)
 
     def edge(target):
@@ -603,13 +604,7 @@
     def _():
         conv[pl.ds(tok, 8), :] = jnp.zeros_like(after)
 
-    grad_g = (
-        taps[2:3, :] * conv[pl.ds(0, tok), :]
-        + taps[1:2, :] * conv[pl.ds(1, tok), :]
-        + taps[0:1, :] * conv[pl.ds(2, tok), :]
-    )
-    gci[...] = (grad_g * in_gate[...].astype(jnp.float32)).astype(jnp.bfloat16)
-    gig[...] = (grad_g * conv_in[...].astype(jnp.float32)).astype(jnp.bfloat16)
+    shifted[...] = conv[...]
 
     @pl.when(s > 0)
     def _():
@@ -620,7 +615,7 @@
     each(1, S, lambda k: direct(k).wait_send())
 
 
-def expert_exchange(S, T, cap, inp, cot, placed, slot_w, out_gate, conv_out, w_gate, w_up, w_down):
+def expert_exchange(S, T, cap, inp, cot, placed, weight, out_gate, conv_out, w_gate, w_up, w_down):
     tok, D = inp.shape
     H = w_down.shape[0]
     TH, Q, SH = T // 2, D // T, S // 2
@@ -677,10 +672,10 @@
         compiler_params=pltpu.CompilerParams(
             collective_id=0, has_side_effects=True, vmem_limit_bytes=67_043_328
         ),
-    )(inp, cot, placed, slot_w, out_gate, conv_out, w_gate, w_up, w_down)
-
-
-def mixer(S, T, placed, cot, out_gate, conv_out, in_gate, conv_in, taps, back, mix_all, w_out):
+    )(inp, cot, placed, weight, out_gate, conv_out, w_gate, w_up, w_down)
+
+
+def mixer(S, T, placed, cot, out_gate, back, mix_all, w_out):
     tok, D = cot.shape
     B = w_out.shape[1]
     cap = placed.shape[1]
@@ -689,13 +684,12 @@
     dma = pltpu.SemaphoreType.DMA
     vmem = pl.BlockSpec(memory_space=pltpu.VMEM)
     hbm = pl.BlockSpec(memory_space=pl.ANY)
-    small = jax.ShapeDtypeStruct((tok, B), bf)
     return pl.pallas_call(
         functools.partial(mixer_kernel, S, T),
         name="mixer",
-        out_shape=(jax.ShapeDtypeStruct((D // S, B), f32), small, small, small),
-        in_specs=[vmem] * 7 + [hbm] * 3,
-        out_specs=(vmem,) * 4,
+        out_shape=tuple(jax.ShapeDtypeStruct((n, B), f32) for n in (D // S, tok, tok + 8)),
+        in_specs=[vmem] * 3 + [hbm] * 3,
+        out_specs=(vmem,) * 3,
         scratch_shapes=[
             pltpu.VMEM((S, cap, Q), bf),
             pltpu.VMEM((S, tok, B), bf),
@@ -720,7 +714,56 @@
         compiler_params=pltpu.CompilerParams(
             collective_id=1, has_side_effects=True, vmem_limit_bytes=67_043_328
         ),
-    )(placed, cot, out_gate, conv_out, in_gate, conv_in, taps, back, mix_all, w_out)
+    )(placed, cot, out_gate, back, mix_all, w_out)
+
+
+def finish_kernel(parts, gm, conv, conv_out, in_gate, conv_in, taps, *refs):
+    n = len(parts)
+    ins, gog, gci, gig, outs = refs[:n], refs[n], refs[n + 1], refs[n + 2], refs[n + 3 : 2 * n + 3]
+    held, insem, outsem = refs[2 * n + 3 : 3 * n + 3], refs[3 * n + 3], refs[3 * n + 4]
+    tok = gm.shape[0]
+    pieces = []
+    for m in range(n):
+        rows = parts[m].shape[0] // CUTS
+        for c in range(CUTS):
+            cut, sem = pl.ds(c * rows, rows), m * CUTS + c
+            take = pltpu.make_async_copy(ins[m].at[cut, :], held[m].at[cut, :], insem.at[sem])
+            give = pltpu.make_async_copy(held[m].at[cut, :], outs[m].at[cut, :], outsem.at[sem])
+            take.start()
+            pieces.append((take, give))
+    for take, give in pieces[: len(pieces) // 2]:
+        take.wait()
+        give.start()
+    grad_g = (
+        taps[2:3, :] * conv[pl.ds(0, tok), :]
+        + taps[1:2, :] * conv[pl.ds(1, tok), :]
+        + taps[0:1, :] * conv[pl.ds(2, tok), :]
+    )
+    gog[...] = (gm[...] * conv_out[...].astype(jnp.float32)).astype(jnp.bfloat16)
+    gci[...] = (grad_g * in_gate[...].astype(jnp.float32)).astype(jnp.bfloat16)
+    gig[...] = (grad_g * conv_in[...].astype(jnp.float32)).astype(jnp.bfloat16)
+    for take, give in pieces[len(pieces) // 2 :]:
+        take.wait()
+        give.start()
+    for _, give in pieces:
+        give.wait()
+
+
+def finish(gm, conv, conv_out, in_gate, conv_in, taps, *parts):
+    vmem = pl.BlockSpec(memory_space=pltpu.VMEM)
+    hbm = pl.BlockSpec(memory_space=pl.ANY)
+    shapes = tuple(jax.ShapeDtypeStruct(part.shape, part.dtype) for part in parts)
+    small = jax.ShapeDtypeStruct(conv_out.shape, conv_out.dtype)
+    return pl.pallas_call(
+        functools.partial(finish_kernel, shapes),
+        name="finish",
+        out_shape=(small, small, small) + shapes,
+        in_specs=[vmem] * 6 + [hbm] * len(parts),
+        out_specs=(vmem,) * 3 + (hbm,) * len(parts),
+        scratch_shapes=[pltpu.VMEM(part.shape, part.dtype) for part in parts]
+        + [pltpu.SemaphoreType.DMA((len(parts) * CUTS,))] * 2,
+        compiler_params=pltpu.CompilerParams(vmem_limit_bytes=67_043_328),
+    )(gm, conv, conv_out, in_gate, conv_in, taps, *parts)
 
 
 def slot_masks(routes, route_weight, experts, capacity):
@@ -735,8 +778,7 @@
     rank = jnp.where(chosen, rank.astype(jnp.int32), -1)
     slots = jnp.arange(capacity, dtype=jnp.int32)
     placed = rank[:, None, :] == slots[None, :, None]
-    slot_weight = jnp.sum(jnp.where(placed, weight[:, None, :], 0.0), axis=2, keepdims=True)
-    return placed.astype(jnp.bfloat16), slot_weight
+    return placed.astype(jnp.bfloat16), weight
 
 
 def per_device(
@@ -747,14 +789,19 @@
     tp_size = lax.axis_size("tp")
     tok_rows, top_k = routes.shape
     capacity = -(-max(2, 2 * tok_rows * top_k // experts) // 16) * 16
-    placed, slot_weight = slot_masks(routes, route_weight, experts, capacity)
+    placed, weight = slot_masks(routes, route_weight, experts, capacity)
     returned, mixed_all, gate_wgrad, up_wgrad, grad_down = expert_exchange(
-        experts, tp_size, capacity, moe_input, cotangent, placed, slot_weight, output_gate, conv_output,
+        experts, tp_size, capacity, moe_input, cotangent, placed, weight, output_gate, conv_output,
         w_gate[0], w_up[0], w_down[0],
     )
-    grad_w_out, grad_conv_input, grad_input_gate, grad_output_gate = mixer(
-        experts, tp_size, placed, cotangent, output_gate, conv_output, input_gate, conv_input, taps,
-        returned, mixed_all, w_out,
+    grad_w_out, grad_mixed, grad_conv = mixer(
+        experts, tp_size, placed, cotangent, output_gate, returned, mixed_all, w_out
+    )
+    (
+        grad_output_gate, grad_conv_input, grad_input_gate, gate_wgrad, up_wgrad, grad_down, grad_w_out
+    ) = finish(
+        grad_mixed, grad_conv, conv_output, input_gate, conv_input, taps,
+        gate_wgrad, up_wgrad, grad_down, grad_w_out,
     )
     return (
         gate_wgrad[None], up_wgrad[None], grad_down[None], grad_w_out,

time: 174 us -> 170 us (0.977)
  local copies, waits for them, and re-layouts: 11.6 us -> 0 us
  Pallas kernels: 158 us -> 166 us
    unnamed x19 -> x0, local copies, waits for them, and re-layouts: 10.6 us -> none
    pallas_call x0 -> x1, Pallas kernels: none -> 8.05 us  [finish(): pl.pallas_call(functools.partial(finish_kernel, shapes), name='finish', o...]
where the time goes in v5:
time: 170 us
  Pallas kernels  166 us (98%)
  other arithmetic  2.84 us (2%)
    pallas_call x1, Pallas kernels, expert_exchange(): pl.pallas_call(functools.partial(expert_kernel, S, T), name='expert_excha...  134 us
    pallas_call x1, Pallas kernels, mixer(): pl.pallas_call(functools.partial(mixer_kernel, S, T), name='mixer', out_s...  24.5 us
    pallas_call x1, Pallas kernels, finish(): pl.pallas_call(functools.partial(finish_kernel, shapes), name='finish', o...  8.05 us

profile of v5, /device:TPU:0, one launch (start us, length us, event | category | flops | bytes accessed | tf_op | source)
XLA Modules:
  0.0 169.7 jit_solution(17949160001942619296)
XLA Ops:
  0.6 0.7 fusion.2
  1.3 0.1 fusion
  1.5 1.3 select_reduce_fusion.weight
  2.8 0.8 fusion.1.placed
  3.6 133.5 %expert_exchange.1 = (bf16[8,96,1024]{2,1,0:T(8,128)(2,1)}, bf16[8,192,512]{2,1,0:T(8,128)(2,1)}, bf16[4096,256]{1,0:T(8,128)(2,1)}, bf16[4096,256]{1,0:T(8,128)(2,1)}, bf16[256,4096]{1,0:T(8,128)(2,1)}) custom-call(bf16[192,4096]{1,0:T(8,128)(2,1)} %inp.1, bf16[192,4096]{1,0:T(8,128)(2,1)} %cot.3, bf16[8,96,192]{2,1,0:T(8,128)(2,1)} %fusion.1.placed, ...), custom_call_target="tpu_custom_call" | custom-call | flops 12884901888 | bytes 50331648 | tf_op jit(solution)/shard_map/expert_exchange/pallas_call | solution.py:627
  137.2 24.5 %mixer.1 = (f32[512,512]{1,0:T(8,128)}, f32[192,512]{1,0:T(8,128)}, f32[200,512]{1,0:T(8,128)}) custom-call(bf16[8,96,192]{2,1,0:T(8,128)(2,1)} %fusion.1.placed, bf16[192,4096]{1,0:T(8,128)(2,1)} %cot.3, bf16[192,512]{1,0:T(8,128)(2,1)} %out_gate.3, bf16[8,96,1024]{2,1,0:T(8,128)(2,1)} %get-tuple-element.22.back_h, ...), custom_call_target="tpu_custom_call" | custom-call | flops 1912602624 | bytes 8388608 | tf_op jit(solution)/shard_map/mixer/pallas_call | solution.py:687
  161.7 8.0 %finish.1 = (bf16[192,512]{1,0:T(8,128)(2,1)}, bf16[192,512]{1,0:T(8,128)(2,1)}, bf16[192,512]{1,0:T(8,128)(2,1)}, bf16[4096,256]{1,0:T(8,128)(2,1)}, bf16[4096,...) custom-call(f32[192,512]{1,0:T(8,128)} %get-tuple-element.24.gm, ...), custom_call_target="tpu_custom_call" | custom-call | tf_op jit(solution)/shard_map/finish/pallas_call | solution.py:757

commit v6 on v5

--- a/solution.py
+++ b/solution.py
@@ -355,6 +355,10 @@
         def _():
             forward(1, then(i))
 
+        @pl.when((i >= 4) & (i < S + 3))
+        def _():
+            reduce_chip(i - 3, then(i - 3))
+
         @pl.when(near_at(i - 1))
         def _():
             forward_on(0, then(i - 1))
@@ -372,10 +376,6 @@
         def _():
             complete(1, then(i - 2))
             gradients(i - 2, then(i - 2))
-
-        @pl.when((i >= 4) & (i < S + 3))
-        def _():
-            reduce_chip(i - 3, then(i - 3))
 
         @pl.when(i >= 6)
         def _():

time: 170 us -> 173 us (1.018)
  Pallas kernels: 166 us -> 169 us
    pallas_call x1, Pallas kernels: 24.5 us -> 26.6 us  [mixer(): pl.pallas_call(functools.partial(mixer_kernel, S, T), name='mixer', out_s...]
where the time goes in v6:
time: 173 us
  Pallas kernels  169 us (98%)
  other arithmetic  2.84 us (2%)
    pallas_call x1, Pallas kernels, expert_exchange(): pl.pallas_call(functools.partial(expert_kernel, S, T), name='expert_excha...  135 us
    pallas_call x1, Pallas kernels, mixer(): pl.pallas_call(functools.partial(mixer_kernel, S, T), name='mixer', out_s...  26.6 us
    pallas_call x1, Pallas kernels, finish(): pl.pallas_call(functools.partial(finish_kernel, shapes), name='finish', o...  8.05 us

profile of v6, /device:TPU:0, one launch (start us, length us, event | category | flops | bytes accessed | tf_op | source)
XLA Modules:
  0.0 173.0 jit_solution(8142151837642588893)
XLA Ops:
  0.6 0.7 fusion.2
  1.3 0.1 fusion
  1.5 1.3 select_reduce_fusion.weight
  2.8 0.8 fusion.1.placed
  3.6 134.8 %expert_exchange.1 = (bf16[8,96,1024]{2,1,0:T(8,128)(2,1)}, bf16[8,192,512]{2,1,0:T(8,128)(2,1)}, bf16[4096,256]{1,0:T(8,128)(2,1)}, bf16[4096,256]{1,0:T(8,128)(2,1)}, bf16[256,4096]{1,0:T(8,128)(2,1)}) custom-call(bf16[192,4096]{1,0:T(8,128)(2,1)} %inp.1, bf16[192,4096]{1,0:T(8,128)(2,1)} %cot.3, bf16[8,96,192]{2,1,0:T(8,128)(2,1)} %fusion.1.placed, ...), custom_call_target="tpu_custom_call" | custom-call | flops 12884901888 | bytes 50331648 | tf_op jit(solution)/shard_map/expert_exchange/pallas_call | solution.py:627
  138.4 26.6 %mixer.1 = (f32[512,512]{1,0:T(8,128)}, f32[192,512]{1,0:T(8,128)}, f32[200,512]{1,0:T(8,128)}) custom-call(bf16[8,96,192]{2,1,0:T(8,128)(2,1)} %fusion.1.placed, bf16[192,4096]{1,0:T(8,128)(2,1)} %cot.3, bf16[192,512]{1,0:T(8,128)(2,1)} %out_gate.3, bf16[8,96,1024]{2,1,0:T(8,128)(2,1)} %get-tuple-element.22.back_h, ...), custom_call_target="tpu_custom_call" | custom-call | flops 1912602624 | bytes 8388608 | tf_op jit(solution)/shard_map/mixer/pallas_call | solution.py:687
  165.0 8.0 %finish.1 = (bf16[192,512]{1,0:T(8,128)(2,1)}, bf16[192,512]{1,0:T(8,128)(2,1)}, bf16[192,512]{1,0:T(8,128)(2,1)}, bf16[4096,256]{1,0:T(8,128)(2,1)}, bf16[4096,...) custom-call(f32[192,512]{1,0:T(8,128)} %get-tuple-element.24.gm, ...), custom_call_target="tpu_custom_call" | custom-call | tf_op jit(solution)/shard_map/finish/pallas_call | solution.py:757
